TPU v7x, 512 devices: a whole 4x4x16 slice. The times are simulated.
512 devices in a mesh: sp: 32 (over z, core), tp: 16 (over y, x).
Axes of the slice: x: 4, y: 4, z: 16, core: 2. Of those that a mesh axis runs over, the one named last changes fastest.
Arguments:
- wide_queries: bfloat16 [2048, 2560], P('sp', 'tp'), may hold values from -512 to 512
- narrow_queries: bfloat16 [2048, 1536], P('sp', 'tp'), may hold values from -512 to 512
- kv_latent: bfloat16 [2048, 512], P('sp'), may hold values from -6 to 6
- rope_key: bfloat16 [2048, 32], P('sp'), may hold values from -4 to 4
- latent_gain: float32 [512], replicated, may hold values from 0.1 to 1.9
- wide_kv_weight: bfloat16 [512, 4096], P(None, 'tp'), may hold values from -0.25 to 0.25
- narrow_kv_weight: bfloat16 [512, 2048], P(None, 'tp'), may hold values from -0.25 to 0.25
- wide_out_weight: bfloat16 [2048, 2048], P('tp'), may hold values from -0.4375 to 0.4375
- narrow_out_weight: bfloat16 [1024, 2048], P('tp'), may hold values from -0.4375 to 0.4375
- residual: bfloat16 [2048, 2048], P('sp'), may hold values from -6 to 6
- norm_gain: float32 [2048], replicated, may hold values from 0.1 to 1.9
- route_ids: int32 [2048, 2], P('sp'), may hold values from 0 to 63, all different within a row; in each aligned block of 64 rows (0 to 63, 64 to 127, ...) at most 3 rows name the same one
- route_weights: float32 [2048, 2], P('sp'), may hold values from 0.3 to 1.3
- expert_gate: bfloat16 [64, 2048, 1024], P('sp', None, 'tp'), may hold values from -0.125 to 0.125
- expert_up: bfloat16 [64, 2048, 1024], P('sp', None, 'tp'), may hold values from -0.125 to 0.125
- expert_down: bfloat16 [64, 1024, 2048], P('sp', 'tp'), may hold values from -0.1875 to 0.1875
- shared_gate: bfloat16 [2048, 1024], P(None, 'tp'), may hold values from -0.125 to 0.125
- shared_up: bfloat16 [2048, 1024], P(None, 'tp'), may hold values from -0.125 to 0.125
- shared_down: bfloat16 [1024, 2048], P('tp'), may hold values from -0.1875 to 0.1875
Outputs:
- mixed_out: bfloat16 [2048, 2048], P('sp', 'tp')
Inputs may be any that keep to these rules, and one draw needn't show every extreme that they name: `route_ids`: in the rows of one index of sp (aligned blocks of 64 rows) no expert is named by more than 3 rows, and some expert by exactly that many; each row names 2 different experts.
All inputs are finite; a program needn't handle non-finite values.
Results may differ from a plain program's by a relative error of at most 0.018.
Values may be sent and summed in bfloat16 or wider, within the bound.
A program may use at most 64 MiB of HBM per device.

v0:
```python
import jax
import jax.numpy as jnp
from jax import lax
from jax.sharding import Mesh
from jax.sharding import PartitionSpec as P

D_MODEL = 2048
WIDE_NOPE = 128
WIDE_VALUE = 128
NARROW_NOPE = 64
NARROW_VALUE = 64
ROPE_DIM = 32
SP = ("sp_0", "sp_1")


THETA = 10000.0
EPS = 1e-06
FLOOR = -1e30


def from_everyone(shard, axis):
    copies = jnp.broadcast_to(shard, (lax.axis_size(axis), *shard.shape))
    return lax.all_to_all(copies, axis, split_axis=0, concat_axis=0, tiled=True)


def in_order(pieces, dim):
    pieces = jnp.moveaxis(pieces, 0, dim)
    shape = pieces.shape
    return pieces.reshape(*shape[:dim], shape[dim] * shape[dim + 1], *shape[dim + 2 :])


def gather_axes(shard, axes, dim):
    far, near = axes
    pieces = from_everyone(from_everyone(shard, far), near)
    return in_order(pieces.swapaxes(0, 1).reshape(-1, *shard.shape), dim)


def in_one_piece(arrays, axis, dim, along):
    ends, at = ([], 0)
    for a in arrays[:-1]:
        at += a.shape[along]
        ends.append(at)
    both = jnp.concatenate(arrays, axis=along)
    return tuple(jnp.split(gather_axes(both, axis, dim), ends, axis=along))


def cut_along(shard, dim, count):
    before, after = (shard.shape[:dim], shard.shape[dim + 1 :])
    return jnp.moveaxis(shard.reshape(*before, count, -1, *after), dim, 0)


def summed_on_arrival(shard, axis, dim):
    pieces = cut_along(shard, dim, lax.axis_size(axis))
    arrived = lax.all_to_all(pieces, axis, split_axis=0, concat_axis=0, tiled=True)
    return arrived.astype(jnp.float32).sum(axis=0)


def padded_to(lines, count):
    spare = -len(lines) % count
    return jnp.pad(lines, [(0, spare)] + [(0, 0)] * (lines.ndim - 1))


def gather_directly(shard, axis, dim):
    return in_order(from_everyone(shard, axis), dim)


def sum_by_parts(shard, axes):
    lines = shard.reshape(-1, shard.shape[-1])
    own = summed_on_arrival(padded_to(lines, lax.axis_size(axes)), axes, 0)
    whole = gather_directly(own.astype(jnp.bfloat16), axes, 0)
    return whole[: len(lines)].reshape(shard.shape).astype(jnp.float32)


def rounded(values):
    return lax.optimization_barrier(values.astype(jnp.bfloat16)).astype(jnp.float32)


def rotate(values, positions):
    half_width = values.shape[-1] // 2
    frequency = THETA ** (-2.0 * jnp.arange(half_width, dtype=jnp.float32) / values.shape[-1])
    angles = positions.astype(jnp.float32)[:, None] * frequency[None, :]
    if values.ndim == 3:
        angles = angles[:, None, :]
    cosine = jnp.cos(angles)
    sine_part = jnp.sin(angles)
    as_float = values.astype(jnp.float32)
    first_half = as_float[..., :half_width]
    second_half = as_float[..., half_width:]
    return jnp.concatenate(
        [
            first_half * cosine - second_half * sine_part,
            second_half * cosine + first_half * sine_part,
        ],
        axis=-1,
    ).astype(jnp.bfloat16)


def rms_scale(values, gain):
    as_float = values.astype(jnp.float32)
    scaled = as_float * lax.rsqrt(jnp.mean(as_float * as_float, axis=-1, keepdims=True) + EPS)
    return (scaled * gain).astype(jnp.bfloat16)


def fresh_state(head_count, query_count, value_width):
    return (
        jnp.full((head_count, query_count), FLOOR, jnp.float32),
        jnp.zeros((head_count, query_count), jnp.float32),
        jnp.zeros((head_count, query_count, value_width), jnp.float32),
    )


def update(carry_part, queries, nope_width, kv_rows, rot_rows, query_pos, key_pos):
    row_peak, row_total, summed = carry_part
    head_count = queries.shape[1]
    key_value = kv_rows.reshape(kv_rows.shape[0], head_count, -1)
    values = key_value[..., nope_width:]
    shared_rot = rot_rows[:, None, :]
    whole_keys = jnp.concatenate([key_value[..., :nope_width], shared_rot], axis=-1)
    scores = jnp.einsum("qhd,khd->hqk", queries, whole_keys, preferred_element_type=jnp.float32)
    scores = scores * queries.shape[-1] ** (-0.5)
    allowed = (query_pos[:, None] >= key_pos[None, :])[None]
    newest = jnp.maximum(row_peak, jnp.max(jnp.where(allowed, scores, FLOOR), axis=-1))
    weights = jnp.where(allowed, jnp.exp(scores - newest[..., None]), 0.0)
    row_total = jnp.sum(weights, axis=-1)
    summed = jnp.einsum(
        "hqk,khv->hqv", weights.astype(jnp.bfloat16), values, preferred_element_type=jnp.float32
    )
    return (newest, row_total, summed)


def local(
    wide_queries,
    narrow_queries,
    kv_latent,
    rope_key,
    latent_gain,
    wide_kv_weight,
    narrow_kv_weight,
    wide_out_weight,
    narrow_out_weight,
    residual,
    norm_gain,
    route_ids,
    route_weights,
    expert_gate,
    expert_up,
    expert_down,
    shared_gate,
    shared_up,
    shared_down,
):
    tok_rows = residual.shape[0]
    positions = lax.axis_index(SP) * tok_rows + jnp.arange(tok_rows, dtype=jnp.int32)
    wide_count = wide_out_weight.shape[0] // WIDE_VALUE
    narrow_count = narrow_out_weight.shape[0] // NARROW_VALUE
    wide_q = wide_queries.reshape(tok_rows, wide_count, WIDE_NOPE + ROPE_DIM)
    wide_q = jnp.concatenate(
        [wide_q[..., :WIDE_NOPE], rotate(wide_q[..., WIDE_NOPE:], positions)], axis=-1
    )
    narrow_q = narrow_queries.reshape(tok_rows, narrow_count, NARROW_NOPE + ROPE_DIM)
    narrow_q = jnp.concatenate(
        [narrow_q[..., :NARROW_NOPE], rotate(narrow_q[..., NARROW_NOPE:], positions)], axis=-1
    )
    key_rot = rotate(rope_key, positions)
    latent = rms_scale(kv_latent, latent_gain)
    initial = (
        fresh_state(wide_count, tok_rows, WIDE_VALUE),
        fresh_state(narrow_count, tok_rows, NARROW_VALUE),
    )
    wide_kv = jnp.dot(latent, wide_kv_weight, preferred_element_type=jnp.float32).astype(
        jnp.bfloat16
    )
    narrow_kv = jnp.dot(latent, narrow_kv_weight, preferred_element_type=jnp.float32).astype(
        jnp.bfloat16
    )
    pieces = in_one_piece((wide_kv, narrow_kv, key_rot), ("sp_0", "sp_1"), 0, 1)
    rot_rows = pieces[2]
    key_pos = jnp.arange(rot_rows.shape[0], dtype=jnp.int32)
    final_state = (
        update(initial[0], wide_q, WIDE_NOPE, pieces[0], rot_rows, positions, key_pos),
        update(initial[1], narrow_q, NARROW_NOPE, pieces[1], rot_rows, positions, key_pos),
    )
    wide_state, narrow_state = final_state
    wide_att = (wide_state[2] / wide_state[1][..., None]).astype(jnp.bfloat16)
    narrow_att = (narrow_state[2] / narrow_state[1][..., None]).astype(jnp.bfloat16)
    partial_proj = jnp.einsum(
        "hqv,hvd->qd",
        wide_att,
        wide_out_weight.reshape(wide_count, WIDE_VALUE, D_MODEL),
        preferred_element_type=jnp.float32,
    )
    partial_proj = partial_proj + jnp.einsum(
        "hqv,hvd->qd",
        narrow_att,
        narrow_out_weight.reshape(narrow_count, NARROW_VALUE, D_MODEL),
        preferred_element_type=jnp.float32,
    )
    proj_sum = sum_by_parts(rounded(partial_proj).astype(jnp.bfloat16), "tp")
    stream = (residual.astype(jnp.float32) + rounded(proj_sum)).astype(jnp.bfloat16)
    normed = rms_scale(stream, norm_gain)
    shared_hidden = (
        jax.nn.silu(jnp.dot(normed, shared_gate, preferred_element_type=jnp.float32))
        * jnp.dot(normed, shared_up, preferred_element_type=jnp.float32)
    ).astype(jnp.bfloat16)
    shared_part = jnp.dot(shared_hidden, shared_down, preferred_element_type=jnp.float32)
    shared_out = rounded(summed_on_arrival(rounded(shared_part).astype(jnp.bfloat16), "tp", 1))
    top_count = route_ids.shape[1]
    local_experts = expert_gate.shape[0]
    sp_count = lax.axis_size(SP)
    expert_total = sp_count * local_experts
    capacity = max(2, 3 * tok_rows * top_count // (2 * expert_total))
    flat_ids = route_ids.reshape(-1)
    one_hot = (flat_ids[:, None] == jnp.arange(expert_total, dtype=jnp.int32)[None, :]).astype(
        jnp.int32
    )
    earlier = jnp.cumsum(one_hot, axis=0) - one_hot
    slot_index = flat_ids * capacity + jnp.sum(earlier * one_hot, axis=1)
    copy_token = jnp.arange(tok_rows * top_count, dtype=jnp.int32) // top_count
    source_row = jnp.zeros((expert_total * capacity,), jnp.int32).at[slot_index].set(copy_token)
    filled = jnp.zeros((expert_total * capacity,), jnp.bfloat16).at[slot_index].set(1.0)
    column_width = D_MODEL // lax.axis_size("tp")
    column_start = lax.axis_index("tp") * column_width
    own_normed = lax.dynamic_slice_in_dim(normed, column_start, column_width, 1)
    outgoing = (own_normed[source_row] * filled[:, None]).reshape(
        sp_count, local_experts, capacity, column_width
    )
    arrived = gather_directly(
        lax.all_to_all(outgoing, SP, split_axis=0, concat_axis=0, tiled=True), "tp", 3
    )
    gate_value = jnp.einsum(
        "sejd,edf->sejf", arrived, expert_gate, preferred_element_type=jnp.float32
    )
    up_value = jnp.einsum("sejd,edf->sejf", arrived, expert_up, preferred_element_type=jnp.float32)
    hidden_units = (jax.nn.silu(gate_value) * up_value).astype(jnp.bfloat16)
    down_part = jnp.einsum(
        "sejf,efd->sejd", hidden_units, expert_down, preferred_element_type=jnp.float32
    )
    expert_result = summed_on_arrival(rounded(down_part).astype(jnp.bfloat16), "tp", 3).astype(
        jnp.bfloat16
    )
    returned = lax.all_to_all(expert_result, SP, split_axis=0, concat_axis=0, tiled=True)
    back_rows = returned.reshape(expert_total * capacity, column_width)[slot_index]
    routed = jnp.sum(
        back_rows.astype(jnp.float32).reshape(tok_rows, top_count, column_width)
        * route_weights[:, :, None],
        axis=1,
    )
    own_stream = lax.dynamic_slice_in_dim(stream, column_start, column_width, 1).astype(jnp.float32)
    return (own_stream + shared_out + routed).astype(jnp.bfloat16)


def solution(mesh):
    torus = Mesh(mesh.devices.reshape(16, 2, mesh.shape["tp"]), ("sp_0", "sp_1", "tp"))
    return jax.shard_map(
        local,
        mesh=torus,
        in_specs=(
            P(SP, "tp"),
            P(SP, "tp"),
            P(SP, None),
            P(SP, None),
            P(),
            P(None, "tp"),
            P(None, "tp"),
            P("tp", None),
            P("tp", None),
            P(SP, None),
            P(),
            P(SP, None),
            P(SP, None),
            P(SP, None, "tp"),
            P(SP, None, "tp"),
            P(SP, "tp", None),
            P(None, "tp"),
            P(None, "tp"),
            P("tp", None),
        ),
        out_specs=P(SP, "tp"),
        check_vma=False,
    )
```

profile of v0, /device:TPU:1, one launch (start us, length us, event | category | flops | bytes accessed | tf_op | source)
XLA Modules:
  0.0 202.4 jit_solution(16078023920893661811)
XLA Ops:
  0.0 1.0 fusion.45
  1.1 0.7 convert_element_type.138
  2.1 1.2 convolution_convert_fusion.3
  3.3 1.2 convolution_convert_fusion.2
  4.6 1.1 broadcast_in_dim.25
  5.7 15.7 %all-to-all-start = ((bf16[16,64,416]{2,1,0:T(8,128)(2,1)}), bf16[16,64,416]{2,1,0:T(8,128)(2,1)S(1)}, u32[]{:S(2)}, u32[]{:S(2)}) async-start(bf16[16,64,416]{2,1,0:T(8,128)(2,1)} %broadcast_in_dim.25), calls=%async_computation | async-start | bytes 2097152 | tf_op jit(solution)/shard_map/all_to_all | solution.py:23
  22.0 0.2 reduce_window_sum.11
  22.2 0.2 select_reduce_fusion.2
  22.5 43.9 %all-to-all-done = bf16[16,64,416]{2,1,0:T(8,128)(2,1)S(1)} async-done(((bf16[16,64,416]{2,1,0:T(8,128)(2,1)}), bf16[16,64,416]{2,1,0:T(8,128)(2,1)S(1)}, u32[]{:S(2)}, u32[]{:S(2)}) %all-to-all-start) | async-done | bytes 852000 | tf_op jit(solution)/shard_map/all_to_all | solution.py:23
  66.4 0.2 broadcast_in_dim.26
  66.7 10.9 %all_to_all.45 = bf16[2,16,64,416]{3,2,1,0:T(8,128)(2,1)S(1)} all-to-all(bf16[2,16,64,416]{3,2,1,0:T(8,128)(2,1)S(1)} %broadcast_in_dim.26), channel_id=1, replica_groups=mesh['sp_0'=16,'sp_1'=2,'tp'=16] {'sp_1'}, dimensions={0} | all-to-all | bytes 3407872 | tf_op jit(solution)/shard_map/all_to_all | solution.py:23
  77.6 0.2 copy.46
  78.1 0.4 convolution_multiply_fusion.1
  78.5 0.6 select_reduce_fusion
  79.2 0.4 fusion.27
  79.6 2.3 %fusion.7 = f32[64,2048]{1,0:T(8,128)} fusion(bf16[128,2048]{1,0:T(8,128)(2,1)} %param.26, bf16[2048,1,256]{2,0,1:T(8,128)(2,1)S(1)} %slice_bitcast_fusion, f32[64,2048]{1,0:T(8,128)S(1)} %convolution_multiply_fusion.1, f32[64]{0:T(128)S(1)} %broadcast_maximum_fusion.1, s32[64]{0:T(128)S(1)} %get-tuple-element.20, f32[64]{0:T(128)S(1)} %get-tuple-element.6), kind=kOutput, calls=%fused_computation.23 | convolution fusion | flops 67649536 | bytes 2098688 | tf_op jit(solution)/shard_map/hqv,hvd->qd/dot_general | solution.py:186
  81.9 1.7 fusion.1
  83.6 0.8 reshape.332
  84.4 6.7 %all-to-all-start.2 = ((bf16[16,4,2048]{2,1,0:T(4,128)(2,1)}), bf16[16,4,2048]{2,1,0:T(4,128)(2,1)S(1)}, u32[]{:S(2)}, u32[]{:S(2)}) async-start(bf16[16,4,2048]{2,1,0:T(4,128)(2,1)} %reshape.332), calls=%async_computation.2 | async-start | bytes 524288 | tf_op jit(solution)/shard_map/all_to_all | solution.py:54
  91.3 0.1 mul.236
  91.4 1.0 scatter_custom_fusion
  92.4 1.3 scatter_custom_fusion.1
  93.8 0.1 mul.238
  93.9 5.4 %all-to-all-done.2 = bf16[16,4,2048]{2,1,0:T(4,128)(2,1)S(1)} async-done(((bf16[16,4,2048]{2,1,0:T(4,128)(2,1)}), bf16[16,4,2048]{2,1,0:T(4,128)(2,1)S(1)}, u32[]{:S(2)}, u32[]{:S(2)}) %all-to-all-start.2) | async-done | bytes 262176 | tf_op jit(solution)/shard_map/all_to_all | solution.py:54
  99.4 0.8 broadcast_in_dim.30
  100.2 3.5 %all-to-all-start.3 = ((bf16[16,4,2048]{2,1,0:T(4,128)(2,1)}), bf16[16,4,2048]{2,1,0:T(4,128)(2,1)S(1)}, u32[]{:S(2)}, u32[]{:S(2)}) async-start(bf16[16,4,2048]{2,1,0:T(4,128)(2,1)} %broadcast_in_dim.30), calls=%async_computation.3 | async-start | bytes 524288 | tf_op jit(solution)/shard_map/all_to_all | solution.py:23
  103.8 7.5 %all-to-all-done.3 = bf16[16,4,2048]{2,1,0:T(4,128)(2,1)S(1)} async-done(((bf16[16,4,2048]{2,1,0:T(4,128)(2,1)}), bf16[16,4,2048]{2,1,0:T(4,128)(2,1)S(1)}, u32[]{:S(2)}, u32[]{:S(2)}) %all-to-all-start.3) | async-done | bytes 262176 | tf_op jit(solution)/shard_map/all_to_all | solution.py:23
  111.3 0.2 fusion.16
  111.7 0.8 gather_fusion
  112.7 22.8 %all_to_all.46 = bf16[32,2,3,128]{3,1,2,0:T(2,128)(2,1)S(1)} all-to-all(bf16[32,2,3,128]{3,1,2,0:T(2,128)(2,1)S(1)} %copy.51), channel_id=1, replica_groups=mesh['sp_0'=16,'sp_1'=2,'tp'=16] {'sp_0','sp_1'}, dimensions={0} | all-to-all | bytes 98304 | tf_op jit(solution)/shard_map/all_to_all | solution.py:228
  135.5 0.2 broadcast_in_dim.34
  135.7 15.1 %all_to_all.47 = bf16[16,32,2,3,128]{4,1,3,2,0:T(8,128)(2,1)S(1)} all-to-all(bf16[16,32,2,3,128]{4,1,3,2,0:T(8,128)(2,1)S(1)} %broadcast_in_dim.34), channel_id=1, replica_groups=mesh['sp_0'=16,'sp_1'=2,'tp'=16] {'tp'}, dimensions={0} | all-to-all | bytes 1572864 | tf_op jit(solution)/shard_map/all_to_all | solution.py:23
  150.9 0.3 convolution_bitcast_fusion.1
  151.2 0.7 fusion
  151.9 1.1 bitcast_bitcast_fusion
  153.0 3.6 %all-to-all-start.7 = ((bf16[16,32,2,3,128]{4,1,3,2,0:T(8,128)(2,1)}), bf16[16,32,2,3,128]{4,1,3,2,0:T(8,128)(2,1)S(1)}, u32[]{:S(2)}, u32[]{:S(2)}) async-start(bf16[16,32,2,3,128]{4,1,3,2,0:T(8,128)(2,1)} %bitcast_bitcast_fusion), calls=%async_computation.7 | async-start | bytes 1572864 | tf_op jit(solution)/shard_map/all_to_all | solution.py:54
  156.7 0.2 fusion.112
  156.9 0.5 convolution_convert_fusion.1
  157.4 0.8 bitcast_bitcast_fusion.1
  158.2 10.2 %all-to-all-done.7 = bf16[16,32,2,3,128]{4,1,3,2,0:T(8,128)(2,1)S(1)} async-done(((bf16[16,32,2,3,128]{4,1,3,2,0:T(8,128)(2,1)}), bf16[16,32,2,3,128]{4,1,3,2,0:T(8,128)(2,1)S(1)}, u32[]{:S(2)}, u32[]{:S(2)}) %all-to-all-start.7) | async-done | bytes 786464 | tf_op jit(solution)/shard_map/all_to_all | solution.py:54
  168.4 3.5 %all-to-all-start.4 = ((bf16[16,64,128]{2,1,0:T(8,128)(2,1)}), bf16[16,64,128]{2,1,0:T(8,128)(2,1)S(1)}, u32[]{:S(2)}, u32[]{:S(2)}) async-start(bf16[16,64,128]{2,1,0:T(8,128)(2,1)} %bitcast_bitcast_fusion.1), calls=%async_computation.4 | async-start | bytes 524288 | tf_op jit(solution)/shard_map/all_to_all | solution.py:54
  172.0 0.7 copy.56
  172.7 6.7 %all-to-all-done.4 = bf16[16,64,128]{2,1,0:T(8,128)(2,1)S(1)} async-done(((bf16[16,64,128]{2,1,0:T(8,128)(2,1)}), bf16[16,64,128]{2,1,0:T(8,128)(2,1)S(1)}, u32[]{:S(2)}, u32[]{:S(2)}) %all-to-all-start.4) | async-done | bytes 262176 | tf_op jit(solution)/shard_map/all_to_all | solution.py:54
  179.4 9.0 %all-to-all-start.8 = ((bf16[32,2,3,128]{3,1,2,0:T(2,128)(2,1)}), bf16[32,2,3,128]{3,1,2,0:T(2,128)(2,1)S(1)}, u32[]{:S(2)}, u32[]{:S(2)}) async-start(bf16[32,2,3,128]{3,1,2,0:T(2,128)(2,1)} %copy.56), calls=%async_computation.8 | async-start | bytes 98304 | tf_op jit(solution)/shard_map/all_to_all | solution.py:241
  188.6 12.2 %all-to-all-done.8 = bf16[32,2,3,128]{3,1,2,0:T(2,128)(2,1)S(1)} async-done(((bf16[32,2,3,128]{3,1,2,0:T(2,128)(2,1)}), bf16[32,2,3,128]{3,1,2,0:T(2,128)(2,1)S(1)}, u32[]{:S(2)}, u32[]{:S(2)}) %all-to-all-start.8) | async-done | bytes 49184 | tf_op jit(solution)/shard_map/all_to_all | solution.py:241
  200.9 0.7 gather_fusion.1
  201.6 0.1 fusion.53
  201.8 0.6 add_convert_fusion.1
  (70 shorter events, 2.4 us)
Async XLA Ops:
  0.0 151.2 %copy-start = (bf16[2,64,2048]{2,1,0:T(8,128)(2,1)S(1)}, bf16[2,64,2048]{2,1,0:T(8,128)(2,1)}, u32[]{:S(2)}) copy-start(bf16[2,64,2048]{2,1,0:T(8,128)(2,1)} %param.34) | copy-start | bytes 1572868
  0.0 21.4 %copy-start.8 = (bf16[64,96]{1,0:T(8,128)(2,1)S(1)}, bf16[64,96]{1,0:T(8,128)(2,1)}, u32[]{:S(2)}) copy-start(bf16[64,96]{1,0:T(8,128)(2,1)} %param.20) | copy-start | bytes 36868
  0.0 21.5 %copy-start.10 = (s32[64,2]{0,1:T(2,128)S(1)}, s32[64,2]{0,1:T(2,128)}, u32[]{:S(2)}) copy-start(s32[64,2]{0,1:T(2,128)} %param.30) | copy-start | bytes 1540
  1.0 20.7 %copy-start.7 = (bf16[64,160]{1,0:T(8,128)(2,1)S(1)}, bf16[64,160]{1,0:T(8,128)(2,1)}, u32[]{:S(2)}) copy-start(bf16[64,160]{1,0:T(8,128)(2,1)} %param.19) | copy-start | bytes 61444
  5.7 60.8 %all-to-all-start = ((bf16[16,64,416]{2,1,0:T(8,128)(2,1)}), bf16[16,64,416]{2,1,0:T(8,128)(2,1)S(1)}, u32[]{:S(2)}, u32[]{:S(2)}) async-start(bf16[16,64,416]{2,1,0:T(8,128)(2,1)} %broadcast_in_dim.25), calls=%async_computation | async-start | bytes 2097152 | tf_op jit(solution)/shard_map/all_to_all | solution.py:23
  79.2 2.7 %copy-start.2 = (bf16[64,2048]{1,0:T(8,128)(2,1)S(1)}, bf16[64,2048]{1,0:T(8,128)(2,1)}, u32[]{:S(2)}) copy-start(bf16[64,2048]{1,0:T(8,128)(2,1)} %param.27) | copy-start | bytes 786436
  81.9 29.4 %copy-start.4 = (bf16[64,2048]{1,0:T(8,128)(2,1)S(1)}, bf16[64,2048]{1,0:T(8,128)(2,1)}, u32[]{:S(2)}) copy-start(bf16[64,2048]{1,0:T(8,128)(2,1)} %param.28) | copy-start | bytes 786436
  83.6 27.9 %copy-start.9 = (f32[2048]{0:T(1024)S(1)}, f32[2048]{0:T(1024)}, u32[]{:S(2)}) copy-start(f32[2048]{0:T(1024)} %param.29) | copy-start | bytes 24580
  84.4 14.9 %all-to-all-start.2 = ((bf16[16,4,2048]{2,1,0:T(4,128)(2,1)}), bf16[16,4,2048]{2,1,0:T(4,128)(2,1)S(1)}, u32[]{:S(2)}, u32[]{:S(2)}) async-start(bf16[16,4,2048]{2,1,0:T(4,128)(2,1)} %reshape.332), calls=%async_computation.2 | async-start | bytes 524288 | tf_op jit(solution)/shard_map/all_to_all | solution.py:54
  100.2 11.0 %all-to-all-start.3 = ((bf16[16,4,2048]{2,1,0:T(4,128)(2,1)}), bf16[16,4,2048]{2,1,0:T(4,128)(2,1)S(1)}, u32[]{:S(2)}, u32[]{:S(2)}) async-start(bf16[16,4,2048]{2,1,0:T(4,128)(2,1)} %broadcast_in_dim.30), calls=%async_computation.3 | async-start | bytes 524288 | tf_op jit(solution)/shard_map/all_to_all | solution.py:23
  111.5 39.3 %copy-start.12 = (bf16[2,2048,64]{1,2,0:T(8,128)(2,1)S(1)}, bf16[2,2048,64]{1,2,0:T(8,128)(2,1)}, u32[]{:S(2)}) copy-start(bf16[2,2048,64]{1,2,0:T(8,128)(2,1)} %param.32) | copy-start | bytes 1572868
  135.5 15.7 %copy-start.1 = (bf16[2,2048,64]{1,2,0:T(8,128)(2,1)S(1)}, bf16[2,2048,64]{1,2,0:T(8,128)(2,1)}, u32[]{:S(2)}) copy-start(bf16[2,2048,64]{1,2,0:T(8,128)(2,1)} %param.33) | copy-start | bytes 1572868
  151.9 4.7 %copy-start.3 = (bf16[2048,64]{0,1:T(8,128)(2,1)S(1)}, bf16[2048,64]{0,1:T(8,128)(2,1)}, u32[]{:S(2)}) copy-start(bf16[2048,64]{0,1:T(8,128)(2,1)} %param.35) | copy-start | bytes 786436
  151.9 5.0 %copy-start.5 = (bf16[64,2048]{1,0:T(8,128)(2,1)S(1)}, bf16[64,2048]{1,0:T(8,128)(2,1)}, u32[]{:S(2)}) copy-start(bf16[64,2048]{1,0:T(8,128)(2,1)} %param.37) | copy-start | bytes 786436
  151.9 5.0 %copy-start.6 = (bf16[2048,64]{0,1:T(8,128)(2,1)S(1)}, bf16[2048,64]{0,1:T(8,128)(2,1)}, u32[]{:S(2)}) copy-start(bf16[2048,64]{0,1:T(8,128)(2,1)} %param.36) | copy-start | bytes 786436
  153.0 15.3 %all-to-all-start.7 = ((bf16[16,32,2,3,128]{4,1,3,2,0:T(8,128)(2,1)}), bf16[16,32,2,3,128]{4,1,3,2,0:T(8,128)(2,1)S(1)}, u32[]{:S(2)}, u32[]{:S(2)}) async-start(bf16[16,32,2,3,128]{4,1,3,2,0:T(8,128)(2,1)} %bitcast_bitcast_fusion), calls=%async_computation.7 | async-start | bytes 1572864 | tf_op jit(solution)/shard_map/all_to_all | solution.py:54
  156.7 31.8 %copy-start.11 = (f32[64,2]{0,1:T(2,128)S(1)}, f32[64,2]{0,1:T(2,128)}, u32[]{:S(2)}) copy-start(f32[64,2]{0,1:T(2,128)} %param.31) | copy-start | bytes 1540
  168.4 11.0 %all-to-all-start.4 = ((bf16[16,64,128]{2,1,0:T(8,128)(2,1)}), bf16[16,64,128]{2,1,0:T(8,128)(2,1)S(1)}, u32[]{:S(2)}, u32[]{:S(2)}) async-start(bf16[16,64,128]{2,1,0:T(8,128)(2,1)} %bitcast_bitcast_fusion.1), calls=%async_computation.4 | async-start | bytes 524288 | tf_op jit(solution)/shard_map/all_to_all | solution.py:54
  179.4 21.4 %all-to-all-start.8 = ((bf16[32,2,3,128]{3,1,2,0:T(2,128)(2,1)}), bf16[32,2,3,128]{3,1,2,0:T(2,128)(2,1)S(1)}, u32[]{:S(2)}, u32[]{:S(2)}) async-start(bf16[32,2,3,128]{3,1,2,0:T(2,128)(2,1)} %copy.56), calls=%async_computation.8 | async-start | bytes 98304 | tf_op jit(solution)/shard_map/all_to_all | solution.py:241
where the time goes:
time: 203 us; the launch traced here: 202 us
  waiting for transfers between devices  85.9 us (42%)
  blocking collectives  48.9 us (24%)
  starting transfers between devices  42.2 us (21%)
  local copies, waits for them, and re-layouts  11.3 us (6%)
  matrix products  9.17 us (5%)
  other arithmetic  4.43 us (2%)
    all_to_all x2, waiting for transfers between devices, from_everyone(): return lax.all_to_all(copies, axis, split_axis=0, concat_axis=0, tiled=True)  51.4 us
    all_to_all x2, blocking collectives, from_everyone(): return lax.all_to_all(copies, axis, split_axis=0, concat_axis=0, tiled=True)  26.1 us
    all_to_all x1, blocking collectives, local(): lax.all_to_all(outgoing, SP, split_axis=0, concat_axis=0, tiled=True)  22.8 us
    all_to_all x3, waiting for transfers between devices, summed_on_arrival(): lax.all_to_all(pieces, axis, split_axis=0, concat_axis=0, tiled=True)  22.2 us
    all_to_all x2, starting transfers between devices, from_everyone(): return lax.all_to_all(copies, axis, split_axis=0, concat_axis=0, tiled=True)  19.3 us
    all_to_all x3, starting transfers between devices, summed_on_arrival(): lax.all_to_all(pieces, axis, split_axis=0, concat_axis=0, tiled=True)  13.9 us
    all_to_all x1, waiting for transfers between devices, local(): lax.all_to_all(expert_result, SP, split_axis=0, concat_axis=0, tiled=True)  12.2 us
    all_to_all x1, starting transfers between devices, local(): lax.all_to_all(expert_result, SP, split_axis=0, concat_axis=0, tiled=True)  9.04 us
  transfers between devices with their start and end apart: 6, of which 6 were waited for; matrix products, arithmetic and copies ran while one was open for 3% of the time, Pallas kernels for 0%

commit v1 on v0

v1 whole, which is shorter than its diff:
```python
import functools

import jax
import jax.numpy as jnp
import numpy as np
from jax import lax
from jax.experimental import pallas as pl
from jax.experimental.pallas import tpu as pltpu
from jax.sharding import Mesh
from jax.sharding import PartitionSpec as P

MESH = pl.DeviceIdType.MESH
ROPE = 32
CAP = 3
SLOTS = 8
THETA = 10000.0
EPS = 1e-06
FLOOR = -1e30
BF = jnp.bfloat16
F32 = jnp.float32


def rotary_table(tokens):
    half = ROPE // 2
    freq = np.float32(THETA) ** (-2.0 * np.arange(half, dtype=np.float32) / np.float32(ROPE))
    freq = freq.astype(np.float32)
    angles = np.arange(tokens, dtype=np.float32)[:, None] * freq[None, :]
    cosine = np.cos(angles.astype(np.float64)).astype(np.float32)
    sine = np.sin(angles.astype(np.float64)).astype(np.float32)
    return np.concatenate([cosine, cosine, -sine, sine], axis=1)


def dot(a, b, ca=1, cb=0):
    return lax.dot_general(a, b, (((ca,), (cb,)), ((), ())), preferred_element_type=F32)


def turned(values, table):
    half = ROPE // 2
    v = values.astype(F32)
    swapped = jnp.concatenate([v[:, half:], v[:, :half]], axis=1)
    return v * table[:, :ROPE] + swapped * table[:, ROPE : 2 * ROPE]


def normalized(values, gain):
    v = values.astype(F32)
    scaled = v * lax.rsqrt(jnp.mean(v * v, axis=-1, keepdims=True) + EPS)
    return (scaled * gain).astype(BF)


def eye(n):
    return lax.broadcasted_iota(jnp.int32, (n, n), 0) == lax.broadcasted_iota(jnp.int32, (n, n), 1)


def upright(line):
    return jnp.sum(jnp.where(eye(line.shape[1]), line, 0.0), axis=1, keepdims=True)


def silu(v):
    return v / (1.0 + jnp.exp(-v))


def shift_of(n):
    return n.bit_length() - 1


def kernel(dims, *refs):
    NZ, NY, NX, TOK, LAT, D, WN, NN = dims
    NT, NS = NY * NX, NZ * 2
    LT, LC, DC = TOK // NY, LAT // NX, D // NT
    KB = NZ * LT
    Q = NS * SLOTS
    RPE = CAP * NS
    ROWS = 2 * RPE
    hbm, out_ref, scratch = refs[:20], refs[20], refs[21:]
    (
        v_wq, v_nq, v_lat, v_rk, v_lg, v_wkv, v_nkv, v_wo, v_no, v_res, v_ng, v_ids, v_rw,
        v_egu, v_ed, v_sgu, v_sd, v_tab,
        latn, rott, zbuf, lat_buf, rot_buf, qlat, qrp, sc,
        pp, rsb, strm, sall, spp, shb, selt, disp, arr, xsend, xall, part, rs2, ret, back,
        lsem, ss, rs, lat_sem,
    ) = scratch
    FF = v_sd.shape[0]
    vmem = [
        v_wq, v_nq, v_lat, v_rk, v_lg, v_wkv, v_nkv, v_wo, v_no, v_res, v_ng, v_ids, v_rw,
        v_egu.at[:, pl.ds(0, FF)], v_egu.at[:, pl.ds(FF, FF)], v_ed,
        v_sgu.at[pl.ds(0, FF)], v_sgu.at[pl.ds(FF, FF)], v_sd, v_tab,
    ]

    z, c = lax.axis_index("z"), lax.axis_index("c")
    y, x = lax.axis_index("y"), lax.axis_index("x")
    t = y * NX + x
    s = z * 2 + c

    def plane(k):
        t2 = (t + k) % NT
        return {"y": t2 // NX, "x": t2 % NX}, t2

    def seq(k):
        s2 = (s + k) % NS
        return {"z": s2 // 2, "c": s2 % 2}, s2

    def cols(i):
        return pl.ds(pl.multiple_of(i * DC, DC), DC)

    def send(src, dst, ssem, rsem, dev):
        pltpu.make_async_remote_copy(
            src_ref=src, dst_ref=dst, send_sem=ssem, recv_sem=rsem, device_id=dev, device_id_type=MESH
        ).start()

    def wait(ref, sem):
        pltpu.make_async_copy(ref, ref, sem).wait()

    def each(lo, hi, f):
        def body(k, carry):
            f(k)
            return carry

        lax.fori_loop(lo, hi, body, 0)

    bar = pltpu.get_barrier_semaphore()
    each(1, NS, lambda k: pl.semaphore_signal(bar, inc=1, device_id=seq(k)[0], device_id_type=MESH))
    each(1, NT, lambda k: pl.semaphore_signal(bar, inc=1, device_id=plane(k)[0], device_id_type=MESH))

    loads = []
    for i in range(20):
        src = hbm[i]
        if i == 9:
            src = src.at[:, cols(t)]
        if i == 19:
            src = src.at[pl.ds(pl.multiple_of(s * TOK, TOK), TOK)]
        loads.append(pltpu.make_async_copy(src, vmem[i], lsem.at[i]))
    for i in (2, 3, 4, 19, 0, 1, 5, 6, 11, 12, 9, 7, 8, 10, 16, 17, 18, 13, 14, 15):
        loads[i].start()

    for i in (2, 3, 4, 19):
        loads[i].wait()
    table = v_tab[...]
    latn[...] = normalized(v_lat[...], v_lg[...])
    rk = turned(dot(v_rk[...], eye(ROPE).astype(BF), 0, 0), table)
    rott[...] = jnp.concatenate([rk[i * LT : (i + 1) * LT] for i in range(NY)], axis=1).astype(BF)

    pl.semaphore_wait(bar, NS + NT - 2)

    own_tile = latn.at[pl.ds(pl.multiple_of(y * LT, LT), LT), pl.ds(pl.multiple_of(x * LC, LC), LC)]
    zslot = zbuf.at[pl.ds(pl.multiple_of(z * LT, LT), LT)]
    rslot = zbuf.at[pl.ds(KB, LT)]

    def z_send(k):
        z2 = (z + k) % NZ
        send(own_tile, zslot, ss.at[0], rs.at[0], {"z": z2})

    def r_send(k):
        z2 = (z + k) % NZ
        send(rott, rslot, ss.at[1], rs.at[1], {"z": z2})

    each(1, NZ, z_send)
    pltpu.make_async_copy(own_tile, zslot, rs.at[0]).start()

    @pl.when(z == t)
    def _():
        each(1, NZ, r_send)
        pltpu.make_async_copy(rott, rslot, rs.at[1]).start()

    for i in (0, 1, 5, 6):
        loads[i].wait()
    wscale, nscale = (WN + ROPE) ** -0.5, (NN + ROPE) ** -0.5
    qlat[:TOK] = (dot(v_wq[:, :WN], v_wkv[:, :WN], 1, 1) * wscale).astype(BF)
    qlat[TOK:] = (dot(v_nq[:, :NN], v_nkv[:, :NN], 1, 1) * nscale).astype(BF)
    qr = jnp.concatenate(
        [turned(v_wq[:, WN:], table) * wscale, turned(v_nq[:, NN:], table) * nscale], axis=0
    )
    for i in range(NY):
        parts = []
        if i:
            parts.append(jnp.zeros((2 * TOK, ROPE * i), F32))
        parts.append(qr)
        if i < NY - 1:
            parts.append(jnp.zeros((2 * TOK, ROPE * (NY - 1 - i)), F32))
        qrp[i] = jnp.concatenate(parts, axis=1).astype(BF)

    for i in (11, 12):
        loads[i].wait()
    lane = lax.broadcasted_iota(jnp.int32, (TOK, Q), 1)
    j = lane & (SLOTS - 1)
    high = (j >= CAP).astype(jnp.int32)
    expert = (lane >> shift_of(SLOTS)) * 2 + high
    hit0 = upright(v_ids[0:1].astype(F32)) == expert.astype(F32)
    hit1 = upright(v_ids[1:2].astype(F32)) == expert.astype(F32)
    ahead = (
        lax.broadcasted_iota(jnp.int32, (TOK, TOK), 0) > lax.broadcasted_iota(jnp.int32, (TOK, TOK), 1)
    ).astype(F32)
    hits = jnp.where(hit0 | hit1, 1.0, 0.0).astype(F32)
    rank = dot(ahead.astype(BF), hits.astype(BF))
    fits = (rank == (j - CAP * high).astype(F32)) & (j < 2 * CAP)
    selt[0] = jnp.where(hit0 & fits, 1.0, 0.0).astype(BF)
    selt[1] = jnp.where(hit1 & fits, 1.0, 0.0).astype(BF)

    wait(zbuf.at[pl.ds(0, KB)], rs.at[0])
    wait(rslot, rs.at[1])
    zlat = zbuf.at[pl.ds(0, KB)]

    def lat_slot(p, t2):
        return lat_buf.at[p, t2 // NX, :, pl.ds(pl.multiple_of((t2 % NX) * LC, LC), LC)]

    my_rot = rot_buf.at[c, pl.ds(pl.multiple_of(t * LT, LT), LT)]
    pltpu.make_async_copy(zlat, lat_slot(c, t), lat_sem.at[0]).start()
    pltpu.make_async_copy(rslot, my_rot, rs.at[2]).start()

    def p_send(k):
        dev, _ = plane(k)
        send(zlat, lat_slot(c, t), ss.at[2], lat_sem.at[k], dev)
        send(rslot, my_rot, ss.at[3], rs.at[2], dev)

    each(1, NT, p_send)
    other = {"c": 1 - c}

    def relay(k):
        t2 = (t + NT - k) % NT
        wait(zlat, lat_sem.at[k])
        send(lat_slot(c, t2), lat_slot(c, t2), ss.at[4], rs.at[3], other)

    each(0, NT, relay)
    wait(rot_buf.at[c], rs.at[2])
    send(rot_buf.at[c], rot_buf.at[c], ss.at[5], rs.at[4], other)
    wait(lat_buf.at[1 - c], rs.at[3])
    wait(rot_buf.at[1 - c], rs.at[4])

    key = lax.broadcasted_iota(jnp.int32, (2 * TOK, KB), 1)
    key_at = (key >> shift_of(LT)) * (2 * TOK) + (key & (LT - 1))
    query_at = s * TOK + (lax.broadcasted_iota(jnp.int32, (2 * TOK, KB), 0) & (TOK - 1))
    ahead_by = query_at - key_at
    peak = jnp.full((2 * TOK, 1), FLOOR, F32)
    ql = qlat[...]
    for p in range(2):
        for i in range(NY):
            scores = dot(ql, lat_buf[p, i], 1, 1) + dot(qrp[i], rot_buf[p], 1, 1)
            scores = jnp.where(ahead_by >= p * TOK + i * LT, scores, FLOOR)
            sc[p * NY + i] = scores
            peak = jnp.maximum(peak, jnp.max(scores, axis=-1, keepdims=True))
    total = jnp.zeros((2 * TOK, 1), F32)
    mixed = jnp.zeros((2 * TOK, LAT), F32)
    for p in range(2):
        for i in range(NY):
            probs = jnp.exp(sc[p * NY + i] - peak)
            total = total + jnp.sum(probs, axis=-1, keepdims=True)
            mixed = mixed + dot(probs.astype(BF), lat_buf[p, i])
    mixed = (mixed / total).astype(BF)
    wide = dot(mixed[:TOK], v_wkv[:, WN:]).astype(BF)
    narrow = dot(mixed[TOK:], v_nkv[...])[:, NN:].astype(BF)
    for i in (7, 8, 9):
        loads[i].wait()
    pp[...] = (dot(wide, v_wo[...]) + dot(narrow, v_no[...])).astype(BF)

    def pp_send(k):
        dev, t2 = plane(k)
        send(pp.at[:, cols(t2)], rsb.at[k - 1], ss.at[6], rs.at[5], dev)

    each(1, NT, pp_send)
    acc = pp[:, cols(t)].astype(F32)
    wait(rsb, rs.at[5])
    for k in range(NT - 1):
        acc = acc + rsb[k].astype(F32)
    stream = (v_res[...].astype(F32) + acc.astype(BF).astype(F32)).astype(BF)
    strm[...] = stream

    sel_all = selt[0] + selt[1]
    disp[...] = dot(sel_all, stream, 0, 0).reshape(NS, SLOTS, DC).astype(BF)

    def d_send(k):
        dev, s2 = seq(k)
        send(disp.at[s2], arr.at[s], ss.at[7], rs.at[6], dev)

    each(1, NS, d_send)
    pltpu.make_async_copy(disp.at[s], arr.at[s], rs.at[6]).start()

    def s_send(k):
        dev, _ = plane(k)
        send(strm, sall.at[:, cols(t)], ss.at[8], rs.at[7], dev)

    each(1, NT, s_send)
    pltpu.make_async_copy(strm, sall.at[:, cols(t)], rs.at[7]).start()

    for i in (10, 16, 17, 18):
        loads[i].wait()
    wait(sall, rs.at[7])
    gain = v_ng[...]
    normed = normalized(sall[...], gain)
    both = dot(normed, v_sgu[...], 1, 1)
    hidden = (silu(both[:, :FF]) * both[:, FF:]).astype(BF)
    spp[...] = dot(hidden, v_sd[...]).astype(BF)

    def sh_send(k):
        dev, t2 = plane(k)
        send(spp.at[:, cols(t2)], shb.at[k - 1], ss.at[9], rs.at[8], dev)

    each(1, NT, sh_send)

    wait(arr, rs.at[6])
    row = lax.broadcasted_iota(jnp.int32, (ROWS, Q), 0)
    slot = lax.broadcasted_iota(jnp.int32, (ROWS, Q), 1)
    pick = jnp.where(slot == (row & (NS - 1)) * SLOTS + (row >> shift_of(NS)), 1.0, 0.0).astype(BF)
    xsend[...] = dot(pick, arr[...].astype(F32).reshape(Q, DC).astype(BF)).astype(BF)

    def x_send(k):
        dev, _ = plane(k)
        send(xsend, xall.at[:, cols(t)], ss.at[10], rs.at[9], dev)

    each(1, NT, x_send)
    pltpu.make_async_copy(xsend, xall.at[:, cols(t)], rs.at[9]).start()
    for i in (13, 14, 15):
        loads[i].wait()
    wait(xall, rs.at[9])
    for e in range(2):
        rows = normalized(xall[e * RPE : (e + 1) * RPE], gain)
        both = dot(rows, v_egu[e], 1, 1)
        hidden = (silu(both[:, :FF]) * both[:, FF:]).astype(BF)
        part[e * RPE : (e + 1) * RPE] = dot(hidden, v_ed[e]).astype(BF)

    def e_send(k):
        dev, t2 = plane(k)
        send(part.at[:, cols(t2)], rs2.at[k - 1], ss.at[11], rs.at[10], dev)

    each(1, NT, e_send)
    acc = part[:, cols(t)].astype(F32)

    shared = spp[:, cols(t)].astype(F32)
    wait(shb, rs.at[8])
    for k in range(NT - 1):
        shared = shared + shb[k].astype(F32)
    shared = shared.astype(BF).astype(F32)

    wait(rs2, rs.at[10])
    for k in range(NT - 1):
        acc = acc + rs2[k].astype(F32)
    row = lax.broadcasted_iota(jnp.int32, (Q, ROWS), 1)
    slot = lax.broadcasted_iota(jnp.int32, (Q, ROWS), 0)
    unpick = jnp.where(slot == (row & (NS - 1)) * SLOTS + (row >> shift_of(NS)), 1.0, 0.0).astype(BF)
    ret[...] = dot(unpick, acc.astype(BF)).reshape(NS, SLOTS, DC).astype(BF)

    def b_send(k):
        dev, s2 = seq(k)
        send(ret.at[s2], back.at[s], ss.at[12], rs.at[11], dev)

    each(1, NS, b_send)
    pltpu.make_async_copy(ret.at[s], back.at[s], rs.at[11]).start()
    wait(back, rs.at[11])
    rows = back[...].astype(F32).reshape(Q, DC).astype(BF)
    routed = dot(selt[0], rows) * upright(v_rw[0:1]) + dot(selt[1], rows) * upright(v_rw[1:2])
    out_ref[...] = (strm[...].astype(F32) + shared + routed).astype(BF)

    wait(zbuf.at[pl.ds(0, (NZ - 1) * LT)], ss.at[0])

    @pl.when(z == t)
    def _():
        wait(zbuf.at[pl.ds(0, (NZ - 1) * LT)], ss.at[1])

    each(1, NT, lambda k: wait(zlat, ss.at[2]))
    wait(rot_buf.at[0, pl.ds(0, (NT - 1) * LT)], ss.at[3])
    wait(lat_buf.at[0], ss.at[4])
    wait(rot_buf.at[0], ss.at[5])
    wait(rsb, ss.at[6])
    wait(disp.at[pl.ds(0, NS - 1)], ss.at[7])
    wait(rsb, ss.at[8])
    wait(shb, ss.at[9])
    wait(rs2, ss.at[10])
    wait(rs2, ss.at[11])
    wait(ret.at[pl.ds(0, NS - 1)], ss.at[12])


def local(dims, interpret, *args):
    NZ, NY, NX, TOK, LAT, D, WN, NN = dims
    NT, NS = NY * NX, NZ * 2
    LT, LC, DC = TOK // NY, LAT // NX, D // NT
    KB = NZ * LT
    Q = NS * SLOTS
    ROWS = 2 * CAP * NS
    args = list(args)
    args[4] = args[4].reshape(1, -1)
    args[10] = args[10].reshape(1, -1)
    for i in (3, 11, 12, 13, 14, 16, 17):
        args[i] = jnp.swapaxes(args[i], -1, -2)
    FF = args[18].shape[0]
    args.append(jnp.asarray(rotary_table(NS * TOK)))
    shapes = [a.shape for a in args]
    shapes[9] = (TOK, DC)
    shapes[19] = (TOK, 2 * ROPE)
    shapes[13] = (2, 2 * FF, D)
    shapes[16] = (2 * FF, D)
    kept = [i for i in range(20) if i not in (14, 17)]
    scratch = [pltpu.VMEM(shapes[i], args[i].dtype) for i in kept]
    scratch += [
        pltpu.VMEM((TOK, LAT), BF),
        pltpu.VMEM((LT, ROPE * NY), BF),
        pltpu.VMEM((KB + LT, LC), BF),
        pltpu.VMEM((2, NY, KB, LAT), BF),
        pltpu.VMEM((2, KB, ROPE * NY), BF),
        pltpu.VMEM((2 * TOK, LAT), BF),
        pltpu.VMEM((NY, 2 * TOK, ROPE * NY), BF),
        pltpu.VMEM((2 * NY, 2 * TOK, KB), F32),
        pltpu.VMEM((TOK, D), BF),
        pltpu.VMEM((NT - 1, TOK, DC), BF),
        pltpu.VMEM((TOK, DC), BF),
        pltpu.VMEM((TOK, D), BF),
        pltpu.VMEM((TOK, D), BF),
        pltpu.VMEM((NT - 1, TOK, DC), BF),
        pltpu.VMEM((2, TOK, Q), BF),
        pltpu.VMEM((NS, SLOTS, DC), BF),
        pltpu.VMEM((NS, SLOTS, DC), BF),
        pltpu.VMEM((ROWS, DC), BF),
        pltpu.VMEM((ROWS, D), BF),
        pltpu.VMEM((ROWS, D), BF),
        pltpu.VMEM((NT - 1, ROWS, DC), BF),
        pltpu.VMEM((NS, SLOTS, DC), BF),
        pltpu.VMEM((NS, SLOTS, DC), BF),
        pltpu.SemaphoreType.DMA((20,)),
        pltpu.SemaphoreType.DMA((13,)),
        pltpu.SemaphoreType.DMA((12,)),
        pltpu.SemaphoreType.DMA((NT,)),
    ]
    return pl.pallas_call(
        functools.partial(kernel, dims),
        out_shape=jax.ShapeDtypeStruct((TOK, DC), BF),
        in_specs=[pl.BlockSpec(memory_space=pl.ANY)] * 20,
        out_specs=pl.BlockSpec(memory_space=pltpu.VMEM),
        scratch_shapes=scratch,
        compiler_params=pltpu.CompilerParams(
            collective_id=0, has_side_effects=True, vmem_limit_bytes=60 * 1024 * 1024
        ),
        name="layer",
    )(*args)


def build(mesh, nz, ny, nx, tok, lat, d, wn, nn):
    torus = Mesh(mesh.devices.reshape(nz, 2, ny, nx), ("z", "c", "y", "x"))
    SP, TP = ("z", "c"), ("y", "x")
    return jax.shard_map(
        functools.partial(local, (nz, ny, nx, tok, lat, d, wn, nn), False),
        mesh=torus,
        in_specs=(
            P(SP, TP),
            P(SP, TP),
            P(SP, None),
            P(SP, None),
            P(),
            P(None, TP),
            P(None, TP),
            P(TP, None),
            P(TP, None),
            P(SP, None),
            P(),
            P(SP, None),
            P(SP, None),
            P(SP, None, TP),
            P(SP, None, TP),
            P(SP, TP, None),
            P(None, TP),
            P(None, TP),
            P(TP, None),
        ),
        out_specs=P(SP, TP),
        check_vma=False,
    )


def solution(mesh):
    return build(mesh, 16, 4, 4, 64, 512, 2048, 128, 64)
```

time: 203 us -> 98.2 us (0.48)
  Pallas kernels: 0 us -> 96.7 us
  waiting for transfers between devices: 85.9 us -> 0 us
  blocking collectives: 48.9 us -> 0 us
  starting transfers between devices: 42.2 us -> 0 us
  local copies, waits for them, and re-layouts: 11.3 us -> 1.32 us
  matrix products: 9.17 us -> 0 us
  other arithmetic: 4.43 us -> 0 us
    pallas_call x0 -> x1, Pallas kernels: none -> 96.7 us  [local(): pl.pallas_call(functools.partial(kernel, dims), out_shape=jax.ShapeDtypeS...]
    all_to_all x6 -> x0, waiting for transfers between devices: 85.9 us -> none  [the longest x2 51.4 us: from_everyone(): return lax.all_to_all(copies, axis, split_axis=0, concat_axis=0, tiled=True)]
    all_to_all x3 -> x0, blocking collectives: 48.9 us -> none  [the longest x2 26.1 us: from_everyone(): return lax.all_to_all(copies, axis, split_axis=0, concat_axis=0, tiled=True)]
    all_to_all x6 -> x0, starting transfers between devices: 42.2 us -> none  [the longest x2 19.3 us: from_everyone(): return lax.all_to_all(copies, axis, split_axis=0, concat_axis=0, tiled=True)]
    dot_general x10 -> x0, matrix products: 9.17 us -> none  [the longest x1 2.31 us: local(): jnp.einsum('hqv,hvd->qd', wide_att, wide_out_weight.reshape(wide_count, W...]
    broadcast_in_dim x6 -> x0, local copies, waits for them, and re-layouts: 2.36 us -> none  [the longest x4 2.29 us: from_everyone(): copies = jnp.broadcast_to(shard, (lax.axis_size(axis), *shard.shape))]
    scatter x2 -> x0, local copies, waits for them, and re-layouts: 2.32 us -> none  [the longest x1 1.34 us: local(): jnp.zeros((expert_total * capacity,), jnp.bfloat16).at[slot_index].set(1.0)]
    reduce_sum x8 -> x0, other arithmetic: 2.18 us -> none  [the longest x2 1.2 us: rms_scale(): jnp.mean(as_float * as_float, axis=-1, keepdims=True) + EPS]
  transfers between devices with their start and end apart: 6 -> 0, of which waited for: 6 -> 0; matrix products, arithmetic and copies ran while one was open for 3% -> 0% of each run, Pallas kernels for 0% -> 0%
where the time goes in v1:
time: 98.2 us; the launch traced here: 98 us
  Pallas kernels  96.7 us (98%)
  local copies, waits for them, and re-layouts  1.32 us (1%)
    pallas_call x1, Pallas kernels, local(): pl.pallas_call(functools.partial(kernel, dims), out_shape=jax.ShapeDtypeS...  96.7 us

profile of v1, /device:TPU:1, one launch (start us, length us, event | category | flops | bytes accessed | tf_op | source)
XLA Modules:
  0.0 98.0 jit_solution(8551395373980483814)
XLA Ops:
  0.0 96.7 %layer.1 = bf16[64,128]{1,0:T(8,128)(2,1)} custom-call(bf16[64,160]{1,0:T(8,128)(2,1)} %refs_0_.1, bf16[64,96]{1,0:T(8,128)(2,1)} %refs_1_.1, bf16[64,512]{1,0:T(8,128)(2,1)} %refs_2_.1, bf16[32,64]{1,0:T(8,128)(2,1)} %bitcast.13, f32[1,512]{1,0:T(1,128)} %bitcast.15, bf16[512,256]{1,0:T(8,128)(2,1)} %refs_5_.1, bf16[512,128]{1,0:T(8,128)(2,1)} %refs_6_.1, ...), custom_call_target="tpu_custom_call" | custom-call | tf_op jit(solution)/shard_map/layer/pallas_call | solution.py:420
  96.7 1.3 %copy.22 = bf16[64,128]{1,0:T(8,128)(2,1)} copy(bf16[64,128]{1,0:T(8,128)(2,1)} %layer.1) | data formatting | bytes 32768

commit v2 on v1

v2 whole, which is shorter than its diff:
```python
import functools

import jax
import jax.numpy as jnp
import numpy as np
from jax import lax
from jax.experimental import pallas as pl
from jax.experimental.pallas import tpu as pltpu
from jax.sharding import Mesh
from jax.sharding import PartitionSpec as P

MESH = pl.DeviceIdType.MESH
ROPE = 32
CAP = 3
SLOTS = 8
THETA = 10000.0
EPS = 1e-06
FLOOR = -1e30
BF = jnp.bfloat16
F32 = jnp.float32


def rotary_table(tokens):
    half = ROPE // 2
    freq = np.float32(THETA) ** (-2.0 * np.arange(half, dtype=np.float32) / np.float32(ROPE))
    freq = freq.astype(np.float32)
    angles = np.arange(tokens, dtype=np.float32)[:, None] * freq[None, :]
    cosine = np.cos(angles.astype(np.float64)).astype(np.float32)
    sine = np.sin(angles.astype(np.float64)).astype(np.float32)
    return np.concatenate([cosine, cosine, -sine, sine], axis=1)


def dot(a, b, ca=1, cb=0):
    return lax.dot_general(a, b, (((ca,), (cb,)), ((), ())), preferred_element_type=F32)


def turned(values, table):
    half = ROPE // 2
    v = values.astype(F32)
    swapped = jnp.concatenate([v[:, half:], v[:, :half]], axis=1)
    return v * table[:, :ROPE] + swapped * table[:, ROPE : 2 * ROPE]


def normalized(values, gain):
    v = values.astype(F32)
    scaled = v * lax.rsqrt(jnp.mean(v * v, axis=-1, keepdims=True) + EPS)
    return (scaled * gain).astype(BF)


def eye(n):
    return lax.broadcasted_iota(jnp.int32, (n, n), 0) == lax.broadcasted_iota(jnp.int32, (n, n), 1)


def upright(line):
    return jnp.sum(jnp.where(eye(line.shape[1]), line, 0.0), axis=1, keepdims=True)


def silu(v):
    return v / (1.0 + jnp.exp(-v))


def shift_of(n):
    return n.bit_length() - 1


def kernel(dims, *refs):
    NZ, NY, NX, TOK, LAT, D, WN, NN, NG = dims
    NT, NS = NY * NX, NZ * 2
    LT, LC, DC = TOK // NY, LAT // NX, D // NT
    GZ = NZ // NG
    CH = GZ * LT
    KB = NY * CH
    HS = NS // NG
    Q = NS * SLOTS
    HQ = HS * SLOTS
    RPE = CAP * HS
    ROWS = 2 * RPE
    hbm, out_ref, scratch = refs[:20], refs[20], refs[21:]
    (
        v_wq, v_nq, v_lat, v_rk, v_lg, v_wkv, v_nkv, v_wo, v_no, v_res, v_ng, v_ids, v_rw,
        v_egu, v_ed, v_sgu, v_sd, v_tab,
        latn, rott, zbuf, zrot, lat_buf, rot_buf, qlat, qrp, mixd,
        pp, rsb, strm, sall, spp, shb, selt, disp, arr, xsend, xall, part, rs2, ret, back,
        lsem, ss, rs, zsem, zsend, rsend, psem, psend, qsem, csem, csend, dsem, dsend, asem, xsem, esem,
    ) = scratch
    FF = v_sd.shape[0]
    vmem = [
        v_wq, v_nq, v_lat, v_rk, v_lg, v_wkv, v_nkv, v_wo, v_no, v_res, v_ng, v_ids, v_rw,
        v_egu.at[0], v_egu.at[1], v_ed,
        v_sgu.at[pl.ds(0, FF)], v_sgu.at[pl.ds(FF, FF)], v_sd, v_tab,
    ]

    z, c = lax.axis_index("z"), lax.axis_index("c")
    y, x = lax.axis_index("y"), lax.axis_index("x")
    t = y * NX + x
    s = z * 2 + c
    gz = lax.div(z, GZ)

    def plane(k):
        t2 = lax.rem(t + k, NT)
        return {"y": lax.div(t2, NX), "x": lax.rem(t2, NX)}, t2

    def seq(k):
        s2 = lax.rem(s + k + NS // 4, NS)
        return {"z": lax.div(s2, 2), "c": lax.rem(s2, 2)}, s2

    def others(f):
        each(0, NS - NS // 4, f)
        each(NS - NS // 4 + 1, NS, f)

    def cols(i):
        return pl.ds(pl.multiple_of(i * DC, DC), DC)

    def send(src, dst, ssem, rsem, dev):
        pltpu.make_async_remote_copy(
            src_ref=src, dst_ref=dst, send_sem=ssem, recv_sem=rsem, device_id=dev, device_id_type=MESH
        ).start()

    def keep(src, dst, sem):
        pltpu.make_async_copy(src, dst, sem).start()

    def wait(ref, sem, name="w"):
        with jax.named_scope(name):
            pltpu.make_async_copy(ref, ref, sem).wait()

    def each(lo, hi, f):
        def body(k, carry):
            f(k)
            return carry

        lax.fori_loop(lo, hi, body, 0)

    bar = pltpu.get_barrier_semaphore()
    others(lambda k: pl.semaphore_signal(bar, inc=1, device_id=seq(k)[0], device_id_type=MESH))
    each(1, NT, lambda k: pl.semaphore_signal(bar, inc=1, device_id=plane(k)[0], device_id_type=MESH))

    loads = []
    for i in range(20):
        src = hbm[i]
        if i == 9:
            src = src.at[:, cols(t)]
        if i == 19:
            src = src.at[pl.ds(pl.multiple_of(s * TOK, TOK), TOK)]
        loads.append(pltpu.make_async_copy(src, vmem[i], lsem.at[i]))
    for i in (2, 3, 4, 19, 0, 1, 5, 6, 11, 12, 9, 7, 8, 10, 16, 17, 18, 13, 14, 15):
        loads[i].start()

    def loaded(*which):
        for i in which:
            loads[i].wait()

    def clear_tile(i):
        zbuf[gz, pl.ds(pl.multiple_of(i * LT, LT), LT)] = jnp.zeros((LT, LC), BF)

    def clear_turn(i):
        rot_buf[c, pl.ds(pl.multiple_of(i * LT, LT), LT)] = jnp.zeros((LT, ROPE * NY), BF)

    each(lax.rem(z, GZ) + 1, GZ, clear_tile)
    each(z + 1, NZ, clear_turn)

    loaded(2, 3, 4, 19)
    table = v_tab[...]
    latn[...] = normalized(v_lat[...], v_lg[...])
    rk = turned(dot(v_rk[...], eye(ROPE).astype(BF), 0, 0), table)
    rott[...] = jnp.concatenate([rk[i * LT : (i + 1) * LT] for i in range(NY)], axis=1).astype(BF)

    with jax.named_scope("w_bar"):
        pl.semaphore_wait(bar, NS + NT - 2)

    own_tile = latn.at[pl.ds(pl.multiple_of(y * LT, LT), LT), pl.ds(pl.multiple_of(x * LC, LC), LC)]
    zslot = zbuf.at[gz, pl.ds(pl.multiple_of(lax.rem(z, GZ) * LT, LT), LT)]

    each(1, NZ - z, lambda k: send(own_tile, zslot, zsend.at[k], zsem.at[z], {"z": z + k}))
    keep(own_tile, zslot, zsem.at[z])

    @pl.when(z == t)
    def _():
        each(1, NZ - z, lambda k: send(rott, zrot, rsend.at[k], rs.at[1], {"z": z + k}))
        keep(rott, zrot, rs.at[1])

    loaded(0, 1, 5, 6)
    wscale, nscale = (WN + ROPE) ** -0.5, (NN + ROPE) ** -0.5
    qlat[:TOK] = (dot(v_wq[:, :WN], v_wkv[:, :WN], 1, 1) * wscale).astype(BF)
    qlat[TOK:] = (dot(v_nq[:, :NN], v_nkv[:, :NN], 1, 1) * nscale).astype(BF)
    qr = jnp.concatenate(
        [turned(v_wq[:, WN:], table) * wscale, turned(v_nq[:, NN:], table) * nscale], axis=0
    )
    qrp[...] = jnp.concatenate([qr] * NY, axis=1).astype(BF)

    def lat_slot(g):
        return lat_buf.at[
            c, g, pl.ds(pl.multiple_of(y * CH, CH), CH), pl.ds(pl.multiple_of(x * LC, LC), LC)
        ]

    top = lax.div(gz, NG - 1)

    def group(k):
        first = lax.div(NG - k, NG)
        second = lax.div(NG + 1 - k, NG) - first
        return top * (first * gz + (1 - first - second) * (NG - k)) + (1 - top) * (gz - k)

    my_rot = rot_buf.at[c, pl.ds(pl.multiple_of(t * LT, LT), LT)]

    def tiles_of(g, k):
        lo = g * GZ
        whole = 1 - lax.div(NG - k, NG)
        return lo, lo + whole * GZ + (1 - whole) * (lax.rem(z, GZ) + 1)

    def group_out(k):
        g = group(k)
        each(*tiles_of(g, k), lambda i: wait(zslot, zsem.at[i], "w_z"))

        @pl.when((lax.div(t, GZ) == g) & (t <= z))
        def _():
            wait(zrot, rs.at[1], "w_zrot")
            keep(zrot, my_rot, qsem.at[t])
            each(1, NT, lambda i: send(zrot, my_rot, ss.at[3], qsem.at[t], plane(i)[0]))

        keep(zbuf.at[g], lat_slot(g), psem.at[g])
        each(1, NT, lambda i: send(zbuf.at[g], lat_slot(g), psend.at[g], psem.at[g], plane(i)[0]))

    each(0, gz + 1, group_out)

    loaded(11, 12)
    lane = lax.broadcasted_iota(jnp.int32, (TOK, Q), 1)
    j = lane & (SLOTS - 1)
    high = (j >= CAP).astype(jnp.int32)
    expert = ((lane >> shift_of(SLOTS)) * 2 + high).astype(F32)
    hit0 = upright(v_ids[0:1].astype(F32)) == expert
    hit1 = upright(v_ids[1:2].astype(F32)) == expert
    ahead = (
        lax.broadcasted_iota(jnp.int32, (TOK, TOK), 0) > lax.broadcasted_iota(jnp.int32, (TOK, TOK), 1)
    ).astype(F32)
    hits = jnp.where(hit0 | hit1, 1.0, 0.0).astype(F32)
    rank = dot(ahead.astype(BF), hits.astype(BF))
    fits = (rank == (j - CAP * high).astype(F32)) & (j < 2 * CAP)
    selt[0] = jnp.where(hit0 & fits, 1.0, 0.0).astype(BF)
    selt[1] = jnp.where(hit1 & fits, 1.0, 0.0).astype(BF)

    other = {"c": 1 - c}

    def turn_rows(p, g):
        return rot_buf.at[p, pl.ds(pl.multiple_of(g * CH, CH), CH)]

    def group_over(k):
        g = group(k)
        wait(lat_buf.at[c, g], psem.at[g], "w_plane")
        send(lat_buf.at[c, g], lat_buf.at[c, g], csend.at[g], csem.at[g], other)
        each(*tiles_of(g, k), lambda i: wait(zrot, qsem.at[i], "w_prot"))
        send(turn_rows(c, g), turn_rows(c, g), dsend.at[g], dsem.at[g], other)

    key = lax.broadcasted_iota(jnp.int32, (2 * TOK, KB), 1)
    key_at = (
        (key >> shift_of(CH)) * LT + ((key >> shift_of(LT)) & (GZ - 1)) * (2 * TOK) + (key & (LT - 1))
    )
    query_at = s * TOK + (lax.broadcasted_iota(jnp.int32, (2 * TOK, KB), 0) & (TOK - 1))
    ahead_by = query_at - key_at
    strip = lax.broadcasted_iota(jnp.int32, (CH, ROPE * NY), 1) >> shift_of(ROPE)
    mixd[...] = jnp.zeros_like(mixd)

    def attend(p, g, carry):
        peak, total = carry
        turns = rot_buf[p, pl.ds(pl.multiple_of(g * CH, CH), CH)].astype(F32)
        turns = jnp.concatenate([jnp.where(strip == i, turns, 0.0) for i in range(NY)], axis=0)
        keys = lat_buf[p, g]
        scores = dot(qlat[...], keys, 1, 1) + dot(qrp[...], turns.astype(BF), 1, 1)
        scores = jnp.where(ahead_by >= p * TOK + g * (GZ * 2 * TOK), scores, FLOOR)
        newest = jnp.maximum(peak, jnp.max(scores, axis=-1, keepdims=True))
        fade = jnp.exp(peak - newest)
        probs = jnp.exp(scores - newest)
        mixd[...] = mixd[...] * fade + dot(probs.astype(BF), keys)
        return newest, total * fade + jnp.sum(probs, axis=-1, keepdims=True)

    def other_attend(k, carry):
        g = group(k)
        wait(lat_buf.at[1 - c, g], csem.at[g], "w_core")
        wait(turn_rows(1 - c, g), dsem.at[g], "w_crot")
        return attend(1 - c, g, carry)

    def both_attend(k, carry):
        group_over(k)
        carry = attend(c, group(k), carry)
        return lax.fori_loop(jnp.maximum(k - 1, 0), k, other_attend, carry)

    carry = (jnp.full((2 * TOK, 1), FLOOR, F32), jnp.zeros((2 * TOK, 1), F32))
    carry = lax.fori_loop(0, gz + 1, both_attend, carry)
    _, total = lax.fori_loop(gz, gz + 1, other_attend, carry)
    mixed = (mixd[...] / total).astype(BF)
    wide = dot(mixed[:TOK], v_wkv[:, WN:]).astype(BF)
    narrow = dot(mixed[TOK:], v_nkv[...])[:, NN:].astype(BF)
    loaded(7, 8, 9)
    pp[...] = (dot(wide, v_wo[...]) + dot(narrow, v_no[...])).astype(BF)

    late = z >= GZ

    def spread(rows, slots, r_axis):
        row = lax.broadcasted_iota(jnp.int32, (rows, slots), r_axis)
        slot = lax.broadcasted_iota(jnp.int32, (rows, slots), 1 - r_axis)
        return jnp.where(slot == (row & (HS - 1)) * SLOTS + (row >> shift_of(HS)), 1.0, 0.0).astype(BF)

    def rows_out(h):
        wait(arr.at[pl.ds(h * HS, HS)], asem.at[h], f"w_arr{h}")
        came = arr[h * HS : (h + 1) * HS].astype(F32).reshape(HQ, DC).astype(BF)
        xsend[h] = dot(spread(ROWS, HQ, 0), came).astype(BF)
        each(1, NT, lambda k: send(xsend.at[h], xall.at[h, :, cols(t)], ss.at[10], xsem.at[h], plane(k)[0]))
        keep(xsend.at[h], xall.at[h, :, cols(t)], xsem.at[h])

    def experts(h):
        wait(xall.at[h], xsem.at[h], f"w_xall{h}")
        both = dot(normalized(xall[h], v_ng[...]), v_egu[...].reshape(4 * FF, D), 1, 1)
        hidden = silu(both[:, : 2 * FF]) * both[:, 2 * FF :]
        first = lax.broadcasted_iota(jnp.int32, (ROWS, 2 * FF), 0) < RPE
        hidden = jnp.where(first == (lax.broadcasted_iota(jnp.int32, (ROWS, 2 * FF), 1) < FF), hidden, 0.0)
        part[h] = dot(hidden.astype(BF), v_ed[...].reshape(2 * FF, D)).astype(BF)

        def e_send(k):
            dev, t2 = plane(k)
            send(part.at[h, :, cols(t2)], rs2.at[h, k - 1], ss.at[11], esem.at[h], dev)

        each(1, NT, e_send)

    def rows_back(h):
        acc = part[h, :, cols(t)].astype(F32)
        wait(rs2.at[h], esem.at[h], f"w_rs2_{h}")
        for k in range(NT - 1):
            acc = acc + rs2[h, k].astype(F32)
        ret[h] = dot(spread(HQ, ROWS, 1), acc.astype(BF)).reshape(HS, SLOTS, DC).astype(BF)

        def b_send(k):
            r2 = lax.rem(s + k, HS)
            s2 = h * HS + r2

            @pl.when(s2 != s)
            def _():
                send(ret.at[h, r2], back.at[s], ss.at[12], rs.at[11], {"z": lax.div(s2, 2), "c": lax.rem(s2, 2)})

            @pl.when(s2 == s)
            def _():
                keep(ret.at[h, r2], back.at[s], rs.at[11])

        each(0, HS, b_send)

    def pp_send(k):
        dev, t2 = plane(k)
        send(pp.at[:, cols(t2)], rsb.at[k - 1], ss.at[6], rs.at[5], dev)

    each(1, NT, pp_send)
    loaded(10, 16, 17, 18, 13, 14, 15)

    @pl.when(late)
    def _():
        rows_out(0)

    acc = pp[:, cols(t)].astype(F32)
    wait(rsb, rs.at[5], "w_proj")
    for k in range(NT - 1):
        acc = acc + rsb[k].astype(F32)
    stream = (v_res[...].astype(F32) + acc.astype(BF).astype(F32)).astype(BF)
    strm[...] = stream

    bunch = lax.div(s, HS)
    disp[...] = dot(selt[0] + selt[1], stream, 0, 0).reshape(NS, SLOTS, DC).astype(BF)

    def d_send(k):
        dev, s2 = seq(k)
        send(disp.at[s2], arr.at[s], ss.at[7], asem.at[bunch], dev)

    others(d_send)
    keep(disp.at[s], arr.at[s], asem.at[bunch])

    def stream_out():
        each(1, NT, lambda k: send(strm, sall.at[:, cols(t)], ss.at[8], rs.at[7], plane(k)[0]))
        keep(strm, sall.at[:, cols(t)], rs.at[7])

    def shared_expert():
        wait(sall, rs.at[7], "w_sall")
        both = dot(normalized(sall[...], v_ng[...]), v_sgu[...], 1, 1)
        hidden = (silu(both[:, :FF]) * both[:, FF:]).astype(BF)
        spp[...] = dot(hidden, v_sd[...]).astype(BF)

    def shared_out():
        def sh_send(k):
            dev, t2 = plane(k)
            send(spp.at[:, cols(t2)], shb.at[k - 1], ss.at[9], rs.at[8], dev)

        each(1, NT, sh_send)

    @pl.when(jnp.logical_not(late))
    def _():
        stream_out()
        shared_expert()
        rows_out(0)
        shared_out()

    rows_out(1)
    experts(0)
    for h in range(2, NG):
        rows_out(h)
    for h in range(1, NG):
        experts(h)
        if h < NG - 1:
            rows_back(h - 1)

    @pl.when(late)
    def _():
        stream_out()

    for h in range(NG - 2, NG):
        rows_back(h)

    @pl.when(late)
    def _():
        shared_expert()
        shared_out()

    shared = spp[:, cols(t)].astype(F32)
    wait(shb, rs.at[8], "w_shb")
    for k in range(NT - 1):
        shared = shared + shb[k].astype(F32)
    before = strm[...].astype(F32) + shared.astype(BF).astype(F32)

    wait(back, rs.at[11], "w_back")
    rows = back[...].astype(F32).reshape(Q, DC).astype(BF)
    routed = dot(selt[0], rows) * upright(v_rw[0:1]) + dot(selt[1], rows) * upright(v_rw[1:2])
    out_ref[...] = (before + routed).astype(BF)

    each(1, NZ - z, lambda k: wait(zslot, zsend.at[k]))

    @pl.when(z == t)
    def _():
        each(1, NZ - z, lambda k: wait(zrot, rsend.at[k]))

    each(0, gz + 1, lambda g: wait(lat_buf.at[0, 0, pl.ds(0, KB * (NT - 1) // NT)], psend.at[g]))

    @pl.when(t <= z)
    def _():
        wait(rot_buf.at[0, pl.ds(0, (NT - 1) * LT)], ss.at[3])

    each(0, gz + 1, lambda g: wait(lat_buf.at[0, 0], csend.at[g]))
    each(0, gz + 1, lambda g: wait(turn_rows(0, 0), dsend.at[g]))
    wait(rsb, ss.at[6])
    wait(disp.at[pl.ds(0, NS - 1)], ss.at[7])
    wait(rsb, ss.at[8])
    wait(shb, ss.at[9])
    wait(rs2, ss.at[10])
    wait(rs2, ss.at[11])
    wait(back.at[pl.ds(0, NS - 1)], ss.at[12])


def local(dims, *args):
    NZ, NY, NX, TOK, LAT, D, WN, NN, NG = dims
    NT, NS = NY * NX, NZ * 2
    LT, LC, DC = TOK // NY, LAT // NX, D // NT
    CH = NZ // NG * LT
    HS = NS // NG
    ROWS = 2 * CAP * HS
    args = list(args)
    args[4] = args[4].reshape(1, -1)
    args[10] = args[10].reshape(1, -1)
    for i in (3, 11, 12, 13, 14, 16, 17):
        args[i] = jnp.swapaxes(args[i], -1, -2)
    FF = args[18].shape[0]
    args.append(jnp.asarray(rotary_table(NS * TOK)))
    shapes = [a.shape for a in args]
    shapes[9] = (TOK, DC)
    shapes[19] = (TOK, 2 * ROPE)
    shapes[13] = (2, 2, FF, D)
    shapes[16] = (2 * FF, D)
    kept = [i for i in range(20) if i not in (14, 17)]
    scratch = [pltpu.VMEM(shapes[i], args[i].dtype) for i in kept]
    scratch += [
        pltpu.VMEM((TOK, LAT), BF),
        pltpu.VMEM((LT, ROPE * NY), BF),
        pltpu.VMEM((NG, CH, LC), BF),
        pltpu.VMEM((LT, ROPE * NY), BF),
        pltpu.VMEM((2, NG, NY * CH, LAT), BF),
        pltpu.VMEM((2, NZ * LT, ROPE * NY), BF),
        pltpu.VMEM((2 * TOK, LAT), BF),
        pltpu.VMEM((2 * TOK, ROPE * NY), BF),
        pltpu.VMEM((2 * TOK, LAT), F32),
        pltpu.VMEM((TOK, D), BF),
        pltpu.VMEM((NT - 1, TOK, DC), BF),
        pltpu.VMEM((TOK, DC), BF),
        pltpu.VMEM((TOK, D), BF),
        pltpu.VMEM((TOK, D), BF),
        pltpu.VMEM((NT - 1, TOK, DC), BF),
        pltpu.VMEM((2, TOK, NS * SLOTS), BF),
        pltpu.VMEM((NS, SLOTS, DC), BF),
        pltpu.VMEM((NS, SLOTS, DC), BF),
        pltpu.VMEM((NG, ROWS, DC), BF),
        pltpu.VMEM((NG, ROWS, D), BF),
        pltpu.VMEM((NG, ROWS, D), BF),
        pltpu.VMEM((NG, NT - 1, ROWS, DC), BF),
        pltpu.VMEM((NG, HS, SLOTS, DC), BF),
        pltpu.VMEM((NS, SLOTS, DC), BF),
        pltpu.SemaphoreType.DMA((20,)),
        pltpu.SemaphoreType.DMA((13,)),
        pltpu.SemaphoreType.DMA((12,)),
        pltpu.SemaphoreType.DMA((NZ,)),
        pltpu.SemaphoreType.DMA((NZ,)),
        pltpu.SemaphoreType.DMA((NZ,)),
        pltpu.SemaphoreType.DMA((NG,)),
        pltpu.SemaphoreType.DMA((NG,)),
        pltpu.SemaphoreType.DMA((NT,)),
        pltpu.SemaphoreType.DMA((NG,)),
        pltpu.SemaphoreType.DMA((NG,)),
        pltpu.SemaphoreType.DMA((NG,)),
        pltpu.SemaphoreType.DMA((NG,)),
        pltpu.SemaphoreType.DMA((NG,)),
        pltpu.SemaphoreType.DMA((NG,)),
        pltpu.SemaphoreType.DMA((NG,)),
    ]
    return pl.pallas_call(
        functools.partial(kernel, dims),
        out_shape=pltpu.VMEM((TOK, DC), BF),
        in_specs=[pl.BlockSpec(memory_space=pltpu.HBM)] * 20,
        out_specs=pl.BlockSpec(memory_space=pltpu.VMEM),
        scratch_shapes=scratch,
        compiler_params=pltpu.CompilerParams(
            collective_id=0, has_side_effects=True, vmem_limit_bytes=60 * 1024 * 1024
        ),
        name="layer",
    )(*args)


def build(mesh, nz, ny, nx, tok, lat, d, wn, nn, ng):
    torus = Mesh(mesh.devices.reshape(nz, 2, ny, nx), ("z", "c", "y", "x"))
    SP, TP = ("z", "c"), ("y", "x")
    return jax.shard_map(
        functools.partial(local, (nz, ny, nx, tok, lat, d, wn, nn, ng)),
        mesh=torus,
        in_specs=(
            P(SP, TP),
            P(SP, TP),
            P(SP, None),
            P(SP, None),
            P(),
            P(None, TP),
            P(None, TP),
            P(TP, None),
            P(TP, None),
            P(SP, None),
            P(),
            P(SP, None),
            P(SP, None),
            P(SP, None, TP),
            P(SP, None, TP),
            P(SP, TP, None),
            P(None, TP),
            P(None, TP),
            P(TP, None),
        ),
        out_specs=P(SP, TP),
        check_vma=False,
    )


def solution(mesh):
    return build(mesh, 16, 4, 4, 64, 512, 2048, 128, 64, 4)
```

time: 98.2 us -> 72.4 us (0.74)
  the two profiles are of different devices: /device:TPU:1 before, /device:TPU:128 now
where the time goes in v2:
time: 72.4 us; the launch traced here: 72.3 us
  Pallas kernels  71.7 us (99%)
    pallas_call x1, Pallas kernels, local(): pl.pallas_call(functools.partial(kernel, dims), out_shape=pltpu.VMEM((TOK...  71.7 us

profile of v2, /device:TPU:128, one launch (start us, length us, event | category | flops | bytes accessed | tf_op | source)
XLA Modules:
  0.0 72.3 jit_solution(2845356258219149304)
XLA Ops:
  0.0 71.7 %layer.1 = bf16[64,128]{1,0:T(8,128)(2,1)S(1)} custom-call(bf16[64,160]{1,0:T(8,128)(2,1)} %refs_0_.1, bf16[64,96]{1,0:T(8,128)(2,1)} %refs_1_.1, bf16[64,512]{1,0:T(8,128)(2,1)} %refs_2_.1, bf16[32,64]{1,0:T(8,128)(2,1)} %bitcast.13, f32[1,512]{1,0:T(1,128)} %bitcast.15, bf16[512,256]{1,0:T(8,128)(2,1)} %refs_5_.1, bf16[512,128]{1,0:T(8,128)(2,1)} %refs_6_.1, ...), custom_call_target="tpu_custom_call" | custom-call | tf_op jit(solution)/shard_map/layer/pallas_call | solution.py:513
  71.7 0.6 copy.22

commit v3 on v2

--- a/solution.py
+++ b/solution.py
@@ -192,12 +192,15 @@
             c, g, pl.ds(pl.multiple_of(y * CH, CH), CH), pl.ds(pl.multiple_of(x * LC, LC), LC)
         ]
 
-    top = lax.div(gz, NG - 1)
+    wrap = lax.div(z, NZ - 2) if NG > 2 else 0
 
     def group(k):
         first = lax.div(NG - k, NG)
         second = lax.div(NG + 1 - k, NG) - first
-        return top * (first * gz + (1 - first - second) * (NG - k)) + (1 - top) * (gz - k)
+        top = lax.div(gz, NG - 1)
+        near = lax.div(NG + 2 - k, NG) - first
+        far_last = first * gz + near * (NG - 2) * (second * (1 - wrap) + (1 - second) * wrap) + (1 - first - near) * 1
+        return top * far_last + (1 - top) * (gz - k) if NG > 2 else gz - k
 
     my_rot = rot_buf.at[c, pl.ds(pl.multiple_of(t * LT, LT), LT)]
 
@@ -346,11 +349,6 @@
 
     each(1, NT, pp_send)
     loaded(10, 16, 17, 18, 13, 14, 15)
-
-    @pl.when(late)
-    def _():
-        rows_out(0)
-
     acc = pp[:, cols(t)].astype(F32)
     wait(rsb, rs.at[5], "w_proj")
     for k in range(NT - 1):
@@ -392,26 +390,32 @@
         rows_out(0)
         shared_out()
 
+    @pl.when(late)
+    def _():
+        rows_out(0)
+        stream_out()
+
     rows_out(1)
     experts(0)
     for h in range(2, NG):
         rows_out(h)
-    for h in range(1, NG):
+    for h in range(1, NG - 1):
         experts(h)
-        if h < NG - 1:
-            rows_back(h - 1)
+        if h == 1:
+            rows_back(0)
 
     @pl.when(late)
     def _():
-        stream_out()
-
-    for h in range(NG - 2, NG):
+        shared_expert()
+
+    experts(NG - 1)
+
+    @pl.when(late)
+    def _():
+        shared_out()
+
+    for h in range(1 if NG > 2 else 0, NG):
         rows_back(h)
-
-    @pl.when(late)
-    def _():
-        shared_expert()
-        shared_out()
 
     shared = spp[:, cols(t)].astype(F32)
     wait(shb, rs.at[8], "w_shb")

time: 72.4 us -> 67.9 us (0.938)
  the two profiles are of different devices: /device:TPU:128 before, /device:TPU:129 now
where the time goes in v3:
time: 67.9 us; the launch traced here: 67.7 us
  Pallas kernels  67.1 us (99%)
    pallas_call x1, Pallas kernels, local(): pl.pallas_call(functools.partial(kernel, dims), out_shape=pltpu.VMEM((TOK...  67.1 us

profile of v3, /device:TPU:129, one launch (start us, length us, event | category | flops | bytes accessed | tf_op | source)
XLA Modules:
  0.0 67.7 jit_solution(8072608463479115967)
XLA Ops:
  0.0 67.1 %layer.1 = bf16[64,128]{1,0:T(8,128)(2,1)S(1)} custom-call(bf16[64,160]{1,0:T(8,128)(2,1)} %refs_0_.1, bf16[64,96]{1,0:T(8,128)(2,1)} %refs_1_.1, bf16[64,512]{1,0:T(8,128)(2,1)} %refs_2_.1, bf16[32,64]{1,0:T(8,128)(2,1)} %bitcast.13, f32[1,512]{1,0:T(1,128)} %bitcast.15, bf16[512,256]{1,0:T(8,128)(2,1)} %refs_5_.1, bf16[512,128]{1,0:T(8,128)(2,1)} %refs_6_.1, ...), custom_call_target="tpu_custom_call" | custom-call | tf_op jit(solution)/shard_map/layer/pallas_call | solution.py:517
  67.1 0.6 copy.22

commit v4 on v3

--- a/solution.py
+++ b/solution.py
@@ -77,15 +77,17 @@
     ROWS = 2 * RPE
     hbm, out_ref, scratch = refs[:20], refs[20], refs[21:]
     (
-        v_wq, v_nq, v_lat, v_rk, v_lg, v_wkv, v_nkv, v_wo, v_no, v_res, v_ng, v_ids, v_rw,
+        v_wq, v_nq, v_lat, v_rk, v_lg, v_wkv, v_nkv, v_wno, v_res, v_ng, v_ids, v_rw,
         v_egu, v_ed, v_sgu, v_sd, v_tab,
         latn, rott, zbuf, zrot, lat_buf, rot_buf, qlat, qrp, mixd,
         pp, rsb, strm, sall, spp, shb, selt, disp, arr, xsend, xall, part, rs2, ret, back,
-        lsem, ss, rs, zsem, zsend, rsend, psem, psend, qsem, csem, csend, dsem, dsend, asem, xsem, esem,
+        lsem, ss, rs, zsem, zsend, rsend, psem, psend, qsem, csem, csend, dsem, dsend, tsem, tsend, asem, xsem, esem,
     ) = scratch
     FF = v_sd.shape[0]
+    WV, NV = hbm[7].shape[0], hbm[8].shape[0]
     vmem = [
-        v_wq, v_nq, v_lat, v_rk, v_lg, v_wkv, v_nkv, v_wo, v_no, v_res, v_ng, v_ids, v_rw,
+        v_wq, v_nq, v_lat, v_rk, v_lg, v_wkv, v_nkv, v_wno.at[pl.ds(0, WV)], v_wno.at[pl.ds(WV, NV)],
+        v_res, v_ng, v_ids, v_rw,
         v_egu.at[0], v_egu.at[1], v_ed,
         v_sgu.at[pl.ds(0, FF)], v_sgu.at[pl.ds(FF, FF)], v_sd, v_tab,
     ]
@@ -188,9 +190,27 @@
     qrp[...] = jnp.concatenate([qr] * NY, axis=1).astype(BF)
 
     def lat_slot(g):
-        return lat_buf.at[
-            c, g, pl.ds(pl.multiple_of(y * CH, CH), CH), pl.ds(pl.multiple_of(x * LC, LC), LC)
-        ]
+        return lat_buf.at[c, g, y, :, x_cols]
+
+    x_cols = pl.ds(pl.multiple_of(x * LC, LC), LC)
+    HC = CH // 2
+    half = (pl.ds(0, HC), pl.ds(HC, HC))
+    two = lax.div(gz, NG - 1)
+
+    def along_x(f):
+        each(1, NX, lambda k: f({"x": lax.rem(x + k, NX)}))
+
+    def along_y(f):
+        each(1, NY, lambda k: f({"y": lax.rem(y + k, NY)}))
+
+    def group_on(k):
+        g = group(k)
+        row = lat_buf.at[c, g, y, half[0], :]
+        wait(row, tsem.at[0, g], "w_step")
+        along_y(lambda dev: send(row, row, tsend.at[2, g], tsem.at[2, g], dev))
+        column = lat_buf.at[c, g, :, half[1], x_cols]
+        wait(column, tsem.at[1, g], "w_step")
+        along_x(lambda dev: send(column, column, tsend.at[3, g], tsem.at[3, g], dev))
 
     wrap = lax.div(z, NZ - 2) if NG > 2 else 0
 
@@ -219,10 +239,29 @@
             keep(zrot, my_rot, qsem.at[t])
             each(1, NT, lambda i: send(zrot, my_rot, ss.at[3], qsem.at[t], plane(i)[0]))
 
-        keep(zbuf.at[g], lat_slot(g), psem.at[g])
-        each(1, NT, lambda i: send(zbuf.at[g], lat_slot(g), psend.at[g], psem.at[g], plane(i)[0]))
-
-    each(0, gz + 1, group_out)
+        @pl.when(two == 0)
+        def _():
+            keep(zbuf.at[g], lat_slot(g), psem.at[g])
+            each(1, NT, lambda i: send(zbuf.at[g], lat_slot(g), psend.at[g], psem.at[g], plane(i)[0]))
+
+        @pl.when(two == 1)
+        def _():
+            for i, along in ((0, along_x), (1, along_y)):
+                src, dst = zbuf.at[g, half[i]], lat_buf.at[c, g, y, half[i], x_cols]
+                keep(src, dst, tsem.at[i, g])
+                along(lambda dev, src=src, dst=dst, i=i: send(src, dst, tsend.at[i, g], tsem.at[i, g], dev))
+
+    each(0, 1, group_out)
+
+    @pl.when(two == 1)
+    def _():
+        each(0, 1, group_on)
+
+    each(1, gz + 1, group_out)
+
+    @pl.when(two == 1)
+    def _():
+        each(1, gz + 1, group_on)
 
     loaded(11, 12)
     lane = lax.broadcasted_iota(jnp.int32, (TOK, Q), 1)
@@ -247,7 +286,16 @@
 
     def group_over(k):
         g = group(k)
-        wait(lat_buf.at[c, g], psem.at[g], "w_plane")
+
+        @pl.when(two == 0)
+        def _():
+            wait(lat_buf.at[c, g], psem.at[g], "w_plane")
+
+        @pl.when(two == 1)
+        def _():
+            wait(lat_buf.at[c, g, pl.ds(0, NY - 1), half[0], :], tsem.at[2, g], "w_plane")
+            wait(lat_buf.at[c, g, :, half[1], pl.ds(0, (NX - 1) * LC)], tsem.at[3, g], "w_plane")
+
         send(lat_buf.at[c, g], lat_buf.at[c, g], csend.at[g], csem.at[g], other)
         each(*tiles_of(g, k), lambda i: wait(zrot, qsem.at[i], "w_prot"))
         send(turn_rows(c, g), turn_rows(c, g), dsend.at[g], dsem.at[g], other)
@@ -261,38 +309,49 @@
     strip = lax.broadcasted_iota(jnp.int32, (CH, ROPE * NY), 1) >> shift_of(ROPE)
     mixd[...] = jnp.zeros_like(mixd)
 
-    def attend(p, g, carry):
-        peak, total = carry
+    def scored(p, g):
         turns = rot_buf[p, pl.ds(pl.multiple_of(g * CH, CH), CH)].astype(F32)
         turns = jnp.concatenate([jnp.where(strip == i, turns, 0.0) for i in range(NY)], axis=0)
-        keys = lat_buf[p, g]
+        keys = lat_buf[p, g].reshape(KB, LAT)
         scores = dot(qlat[...], keys, 1, 1) + dot(qrp[...], turns.astype(BF), 1, 1)
-        scores = jnp.where(ahead_by >= p * TOK + g * (GZ * 2 * TOK), scores, FLOOR)
-        newest = jnp.maximum(peak, jnp.max(scores, axis=-1, keepdims=True))
+        return jnp.where(ahead_by >= p * TOK + g * (GZ * 2 * TOK), scores, FLOOR)
+
+    def attend(places, carry):
+        peak, total = carry
+        scores = [scored(p, g) for p, g in places]
+        newest = peak
+        for sc in scores:
+            newest = jnp.maximum(newest, jnp.max(sc, axis=-1, keepdims=True))
         fade = jnp.exp(peak - newest)
-        probs = jnp.exp(scores - newest)
-        mixd[...] = mixd[...] * fade + dot(probs.astype(BF), keys)
-        return newest, total * fade + jnp.sum(probs, axis=-1, keepdims=True)
-
-    def other_attend(k, carry):
+        mixed, total = mixd[...] * fade, total * fade
+        for (p, g), sc in zip(places, scores):
+            probs = jnp.exp(sc - newest)
+            total = total + jnp.sum(probs, axis=-1, keepdims=True)
+            mixed = mixed + dot(probs.astype(BF), lat_buf[p, g].reshape(KB, LAT))
+        mixd[...] = mixed
+        return newest, total
+
+    def wait_other(k):
         g = group(k)
         wait(lat_buf.at[1 - c, g], csem.at[g], "w_core")
         wait(turn_rows(1 - c, g), dsem.at[g], "w_crot")
-        return attend(1 - c, g, carry)
 
     def both_attend(k, carry):
         group_over(k)
-        carry = attend(c, group(k), carry)
-        return lax.fori_loop(jnp.maximum(k - 1, 0), k, other_attend, carry)
+        wait_other(k - 1)
+        return attend([(c, group(k)), (1 - c, group(k - 1))], carry)
 
     carry = (jnp.full((2 * TOK, 1), FLOOR, F32), jnp.zeros((2 * TOK, 1), F32))
-    carry = lax.fori_loop(0, gz + 1, both_attend, carry)
-    _, total = lax.fori_loop(gz, gz + 1, other_attend, carry)
+    group_over(0)
+    carry = attend([(c, gz)], carry)
+    carry = lax.fori_loop(1, gz + 1, both_attend, carry)
+    wait_other(gz)
+    _, total = attend([(1 - c, group(gz))], carry)
     mixed = (mixd[...] / total).astype(BF)
-    wide = dot(mixed[:TOK], v_wkv[:, WN:]).astype(BF)
-    narrow = dot(mixed[TOK:], v_nkv[...])[:, NN:].astype(BF)
+    wide = dot(mixed[:TOK], v_wkv[:, WN:])
+    narrow = dot(mixed[TOK:], v_nkv[...])[:, NN:]
     loaded(7, 8, 9)
-    pp[...] = (dot(wide, v_wo[...]) + dot(narrow, v_no[...])).astype(BF)
+    pp[...] = dot(jnp.concatenate([wide, narrow], axis=1).astype(BF), v_wno[...]).astype(BF)
 
     late = z >= GZ
 
@@ -386,8 +445,8 @@
     @pl.when(jnp.logical_not(late))
     def _():
         stream_out()
+        rows_out(0)
         shared_expert()
-        rows_out(0)
         shared_out()
 
     @pl.when(late)
@@ -403,20 +462,52 @@
         experts(h)
         if h == 1:
             rows_back(0)
+    experts(NG - 1)
+    for h in range(1 if NG > 2 else 0, NG - 1):
+        rows_back(h)
 
     @pl.when(late)
     def _():
         shared_expert()
-
-    experts(NG - 1)
-
-    @pl.when(late)
-    def _():
         shared_out()
 
-    for h in range(1 if NG > 2 else 0, NG):
-        rows_back(h)
-
+    rows_back(NG - 1)
+
+    each(1, NZ - z, lambda k: wait(zslot, zsend.at[k]))
+
+    @pl.when(z == t)
+    def _():
+        each(1, NZ - z, lambda k: wait(zrot, rsend.at[k]))
+
+    chunks = rsb if CH * LC == TOK * DC else lat_buf.at[0, 0, :, pl.ds(0, CH * (NT - 1) // NT)]
+
+    @pl.when(two == 0)
+    def _():
+        each(0, gz + 1, lambda g: wait(chunks, psend.at[g]))
+
+    @pl.when(two == 1)
+    def _():
+        def left(g):
+            wait(lat_buf.at[0, 0, 0, half[0], pl.ds(0, (NX - 1) * LC)], tsend.at[0, g])
+            wait(lat_buf.at[0, 0, pl.ds(0, NY - 1), half[0], pl.ds(0, LC)], tsend.at[1, g])
+            wait(lat_buf.at[0, 0, pl.ds(0, NY - 1), half[0], :], tsend.at[2, g])
+            wait(lat_buf.at[0, 0, :, half[0], pl.ds(0, (NX - 1) * LC)], tsend.at[3, g])
+
+        each(0, gz + 1, left)
+
+    @pl.when(t <= z)
+    def _():
+        wait(rot_buf.at[0, pl.ds(0, (NT - 1) * LT)], ss.at[3])
+
+    each(0, gz + 1, lambda g: wait(lat_buf.at[0, 0], csend.at[g]))
+    each(0, gz + 1, lambda g: wait(turn_rows(0, 0), dsend.at[g]))
+    wait(rsb, ss.at[6])
+    wait(disp.at[pl.ds(0, NS - 1)], ss.at[7])
+    wait(rsb, ss.at[8])
+    wait(rs2, ss.at[10])
+    wait(rs2, ss.at[11])
+
+    first_weight, second_weight = upright(v_rw[0:1]), upright(v_rw[1:2])
     shared = spp[:, cols(t)].astype(F32)
     wait(shb, rs.at[8], "w_shb")
     for k in range(NT - 1):
@@ -425,29 +516,9 @@
 
     wait(back, rs.at[11], "w_back")
     rows = back[...].astype(F32).reshape(Q, DC).astype(BF)
-    routed = dot(selt[0], rows) * upright(v_rw[0:1]) + dot(selt[1], rows) * upright(v_rw[1:2])
+    routed = dot(selt[0], rows) * first_weight + dot(selt[1], rows) * second_weight
     out_ref[...] = (before + routed).astype(BF)
-
-    each(1, NZ - z, lambda k: wait(zslot, zsend.at[k]))
-
-    @pl.when(z == t)
-    def _():
-        each(1, NZ - z, lambda k: wait(zrot, rsend.at[k]))
-
-    each(0, gz + 1, lambda g: wait(lat_buf.at[0, 0, pl.ds(0, KB * (NT - 1) // NT)], psend.at[g]))
-
-    @pl.when(t <= z)
-    def _():
-        wait(rot_buf.at[0, pl.ds(0, (NT - 1) * LT)], ss.at[3])
-
-    each(0, gz + 1, lambda g: wait(lat_buf.at[0, 0], csend.at[g]))
-    each(0, gz + 1, lambda g: wait(turn_rows(0, 0), dsend.at[g]))
-    wait(rsb, ss.at[6])
-    wait(disp.at[pl.ds(0, NS - 1)], ss.at[7])
-    wait(rsb, ss.at[8])
     wait(shb, ss.at[9])
-    wait(rs2, ss.at[10])
-    wait(rs2, ss.at[11])
     wait(back.at[pl.ds(0, NS - 1)], ss.at[12])
 
 
@@ -470,14 +541,15 @@
     shapes[19] = (TOK, 2 * ROPE)
     shapes[13] = (2, 2, FF, D)
     shapes[16] = (2 * FF, D)
-    kept = [i for i in range(20) if i not in (14, 17)]
+    shapes[7] = (shapes[7][0] + shapes[8][0], D)
+    kept = [i for i in range(20) if i not in (8, 14, 17)]
     scratch = [pltpu.VMEM(shapes[i], args[i].dtype) for i in kept]
     scratch += [
         pltpu.VMEM((TOK, LAT), BF),
         pltpu.VMEM((LT, ROPE * NY), BF),
         pltpu.VMEM((NG, CH, LC), BF),
         pltpu.VMEM((LT, ROPE * NY), BF),
-        pltpu.VMEM((2, NG, NY * CH, LAT), BF),
+        pltpu.VMEM((2, NG, NY, CH, LAT), BF),
         pltpu.VMEM((2, NZ * LT, ROPE * NY), BF),
         pltpu.VMEM((2 * TOK, LAT), BF),
         pltpu.VMEM((2 * TOK, ROPE * NY), BF),
@@ -510,6 +582,8 @@
         pltpu.SemaphoreType.DMA((NG,)),
         pltpu.SemaphoreType.DMA((NG,)),
         pltpu.SemaphoreType.DMA((NG,)),
+        pltpu.SemaphoreType.DMA((4, NG)),
+        pltpu.SemaphoreType.DMA((4, NG)),
         pltpu.SemaphoreType.DMA((NG,)),
         pltpu.SemaphoreType.DMA((NG,)),
         pltpu.SemaphoreType.DMA((NG,)),

time: 67.9 us -> 66.4 us (0.978)
  the two profiles are of different devices: /device:TPU:129 before, /device:TPU:1 now
where the time goes in v4:
time: 66.4 us; the launch traced here: 65.9 us
  Pallas kernels  65.3 us (98%)
    pallas_call x1, Pallas kernels, local(): pl.pallas_call(functools.partial(kernel, dims), out_shape=pltpu.VMEM((TOK...  65.3 us

profile of v4, /device:TPU:1, one launch (start us, length us, event | category | flops | bytes accessed | tf_op | source)
XLA Modules:
  0.0 65.9 jit_solution(2772269584056739100)
XLA Ops:
  0.0 65.3 %layer.1 = bf16[64,128]{1,0:T(8,128)(2,1)S(1)} custom-call(bf16[64,160]{1,0:T(8,128)(2,1)} %refs_0_.1, bf16[64,96]{1,0:T(8,128)(2,1)} %refs_1_.1, bf16[64,512]{1,0:T(8,128)(2,1)} %refs_2_.1, bf16[32,64]{1,0:T(8,128)(2,1)} %bitcast.13, f32[1,512]{1,0:T(1,128)} %bitcast.15, bf16[512,256]{1,0:T(8,128)(2,1)} %refs_5_.1, bf16[512,128]{1,0:T(8,128)(2,1)} %refs_6_.1, ...), custom_call_target="tpu_custom_call" | custom-call | tf_op jit(solution)/shard_map/layer/pallas_call | solution.py:591
  65.3 0.6 copy.22

commit v5 on v4

--- a/solution.py
+++ b/solution.py
@@ -80,7 +80,7 @@
         v_wq, v_nq, v_lat, v_rk, v_lg, v_wkv, v_nkv, v_wno, v_res, v_ng, v_ids, v_rw,
         v_egu, v_ed, v_sgu, v_sd, v_tab,
         latn, rott, zbuf, zrot, lat_buf, rot_buf, qlat, qrp, mixd,
-        pp, rsb, strm, sall, spp, shb, selt, disp, arr, xsend, xall, part, rs2, ret, back,
+        pp, rsb, strm, sall, spp, shb, selt, disp, arr, xsend, xall, part, rs2, ret, back, v_wt,
         lsem, ss, rs, zsem, zsend, rsend, psem, psend, qsem, csem, csend, dsem, dsend, tsem, tsend, asem, xsem, esem,
     ) = scratch
     FF = v_sd.shape[0]
@@ -126,11 +126,19 @@
             pltpu.make_async_copy(ref, ref, sem).wait()
 
     def each(lo, hi, f):
+        run = 1
+        if isinstance(lo, int) and isinstance(hi, int):
+            run = max([u for u in range(1, 8) if (hi - lo) % u == 0], default=1)
+
         def body(k, carry):
-            f(k)
+            for i in range(run):
+                f(lo + k * run + i if run > 1 else k)
             return carry
 
-        lax.fori_loop(lo, hi, body, 0)
+        if run > 1:
+            lax.fori_loop(0, (hi - lo) // run, body, 0)
+        else:
+            lax.fori_loop(lo, hi, body, 0)
 
     bar = pltpu.get_barrier_semaphore()
     others(lambda k: pl.semaphore_signal(bar, inc=1, device_id=seq(k)[0], device_id_type=MESH))
@@ -369,7 +377,7 @@
 
     def experts(h):
         wait(xall.at[h], xsem.at[h], f"w_xall{h}")
-        both = dot(normalized(xall[h], v_ng[...]), v_egu[...].reshape(4 * FF, D), 1, 1)
+        both = dot(normalized(xall[h], v_ng[...]), v_wt[...])
         hidden = silu(both[:, : 2 * FF]) * both[:, 2 * FF :]
         first = lax.broadcasted_iota(jnp.int32, (ROWS, 2 * FF), 0) < RPE
         hidden = jnp.where(first == (lax.broadcasted_iota(jnp.int32, (ROWS, 2 * FF), 1) < FF), hidden, 0.0)
@@ -408,6 +416,7 @@
 
     each(1, NT, pp_send)
     loaded(10, 16, 17, 18, 13, 14, 15)
+    v_wt[...] = v_egu[...].reshape(4 * FF, D).T
     acc = pp[:, cols(t)].astype(F32)
     wait(rsb, rs.at[5], "w_proj")
     for k in range(NT - 1):
@@ -516,7 +525,8 @@
 
     wait(back, rs.at[11], "w_back")
     rows = back[...].astype(F32).reshape(Q, DC).astype(BF)
-    routed = dot(selt[0], rows) * first_weight + dot(selt[1], rows) * second_weight
+    picked = dot(selt[...].reshape(2 * TOK, Q), rows)
+    routed = picked[:TOK] * first_weight + picked[TOK:] * second_weight
     out_ref[...] = (before + routed).astype(BF)
     wait(shb, ss.at[9])
     wait(back.at[pl.ds(0, NS - 1)], ss.at[12])
@@ -569,6 +579,7 @@
         pltpu.VMEM((NG, NT - 1, ROWS, DC), BF),
         pltpu.VMEM((NG, HS, SLOTS, DC), BF),
         pltpu.VMEM((NS, SLOTS, DC), BF),
+        pltpu.VMEM((D, 4 * FF), BF),
         pltpu.SemaphoreType.DMA((20,)),
         pltpu.SemaphoreType.DMA((13,)),
         pltpu.SemaphoreType.DMA((12,)),

time: 66.4 us -> 65.9 us (level)
  no operation moved by 1% of the time
where the time goes in v5:
time: 65.9 us; the launch traced here: 65.3 us
  Pallas kernels  64.7 us (98%)
    pallas_call x1, Pallas kernels, local(): pl.pallas_call(functools.partial(kernel, dims), out_shape=pltpu.VMEM((TOK...  64.7 us

profile of v5, /device:TPU:1, one launch (start us, length us, event | category | flops | bytes accessed | tf_op | source)
XLA Modules:
  0.0 65.3 jit_solution(6907817276584652794)
XLA Ops:
  0.0 64.7 %layer.1 = bf16[64,128]{1,0:T(8,128)(2,1)S(1)} custom-call(bf16[64,160]{1,0:T(8,128)(2,1)} %refs_0_.1, bf16[64,96]{1,0:T(8,128)(2,1)} %refs_1_.1, bf16[64,512]{1,0:T(8,128)(2,1)} %refs_2_.1, bf16[32,64]{1,0:T(8,128)(2,1)} %bitcast.13, f32[1,512]{1,0:T(1,128)} %bitcast.15, bf16[512,256]{1,0:T(8,128)(2,1)} %refs_5_.1, bf16[512,128]{1,0:T(8,128)(2,1)} %refs_6_.1, ...), custom_call_target="tpu_custom_call" | custom-call | tf_op jit(solution)/shard_map/layer/pallas_call | solution.py:602
  64.7 0.6 copy.22

commit v6 on v5

--- a/solution.py
+++ b/solution.py
@@ -180,7 +180,7 @@
     own_tile = latn.at[pl.ds(pl.multiple_of(y * LT, LT), LT), pl.ds(pl.multiple_of(x * LC, LC), LC)]
     zslot = zbuf.at[gz, pl.ds(pl.multiple_of(lax.rem(z, GZ) * LT, LT), LT)]
 
-    each(1, NZ - z, lambda k: send(own_tile, zslot, zsend.at[k], zsem.at[z], {"z": z + k}))
+    each(1, NZ - z, lambda k: send(own_tile, zslot, zsend.at[k], zsem.at[z], {"z": NZ - k}))
     keep(own_tile, zslot, zsem.at[z])
 
     @pl.when(z == t)

time: 65.9 us -> 66.2 us (level)
  no operation moved by 1% of the time
where the time goes in v6:
time: 66.2 us; the launch traced here: 65.7 us
  Pallas kernels  65.1 us (98%)
    pallas_call x1, Pallas kernels, local(): pl.pallas_call(functools.partial(kernel, dims), out_shape=pltpu.VMEM((TOK...  65.1 us

profile of v6, /device:TPU:1, one launch (start us, length us, event | category | flops | bytes accessed | tf_op | source)
XLA Modules:
  0.0 65.7 jit_solution(14023582081462648286)
XLA Ops:
  0.0 65.1 %layer.1 = bf16[64,128]{1,0:T(8,128)(2,1)S(1)} custom-call(bf16[64,160]{1,0:T(8,128)(2,1)} %refs_0_.1, bf16[64,96]{1,0:T(8,128)(2,1)} %refs_1_.1, bf16[64,512]{1,0:T(8,128)(2,1)} %refs_2_.1, bf16[32,64]{1,0:T(8,128)(2,1)} %bitcast.13, f32[1,512]{1,0:T(1,128)} %bitcast.15, bf16[512,256]{1,0:T(8,128)(2,1)} %refs_5_.1, bf16[512,128]{1,0:T(8,128)(2,1)} %refs_6_.1, ...), custom_call_target="tpu_custom_call" | custom-call | tf_op jit(solution)/shard_map/layer/pallas_call | solution.py:602
  65.1 0.6 copy.22
